TPU v7x, 512 devices: a whole 4x4x16 slice. The times are simulated.
512 devices in a mesh: ra: 64 (over z, y), cb: 8 (over x, core).
Axes of the slice: x: 4, y: 4, z: 16, core: 2. Of those that a mesh axis runs over, the one named last changes fastest.
Arguments:
- activations: bfloat16 [768, 4096], P('ra', 'cb'), may hold values from -230 to 230
- gain_first: float32 [4096], P('cb'), may hold values from 0.1 to 1.9
- gate_weight: float32 [11264, 4096], P('ra', 'cb'), may hold values from -0.25 to 0.25
- gate_scale: float32 [11264], P('ra'), may hold values from 0.5 to 2
- up_weight: float32 [11264, 4096], P('ra', 'cb'), may hold values from -0.25 to 0.25
- up_scale: float32 [11264], P('ra'), may hold values from 0.5 to 2
- down_weight: float32 [11264, 4096], P('ra', 'cb'), may hold values from -0.0546875 to 0.0546875
- down_scale: float32 [4096], P('cb'), may hold values from 0.35 to 2.8
- gain_second: float32 [4096], P('cb'), may hold values from 0.1 to 1.9
Outputs:
- normed: bfloat16 [768, 4096], P('ra', 'cb')
All inputs are finite; a program needn't handle non-finite values.
Results may differ from a plain program's by a relative error of at most 0.011.
Values may be sent and summed in bfloat16 or wider, within the bound.
No kernel may reach another device: no remote copies, remote signals or barrier semaphores. Data moves between devices by JAX's collectives and lax.ppermute only.
A program may use at most 64 MiB of HBM per device.

v0:
```python
import jax
import jax.numpy as jnp
from jax import lax
from jax.sharding import Mesh
from jax.sharding import PartitionSpec as P

RA = ("ra_0", "ra_1")


EPS = 1e-06


def gathered_by_axis(value, axes, dim):
    for axis in reversed(axes):
        value = lax.all_gather(value, axis, axis=dim, tiled=True)
    return value


def from_everyone(value, axis):
    peers = lax.axis_size(axis)
    return lax.all_to_all(
        jnp.broadcast_to(value[None], (peers, *value.shape)), axis, 0, 0, tiled=True
    )


def over_copies(value, axis):
    everything = from_everyone(value, axis)
    return jnp.sum(everything.astype(jnp.float32), axis=0)


def split_up(value, dim, peers):
    before, after = (value.shape[:dim], value.shape[dim + 1 :])
    return jnp.moveaxis(value.reshape(*before, peers, -1, *after), dim, 0)


def summed_on_arrival(value, axis, dim):
    peers = lax.axis_size(axis)
    blocks = lax.all_to_all(split_up(value, dim, peers), axis, 0, 0, tiled=True)
    return jnp.sum(blocks.astype(jnp.float32), axis=0)


def of_everyone(value, axis):
    everything = from_everyone(value, axis)
    return jnp.sum(everything, axis=0)


def per_device(
    activations,
    gain_first,
    gate_weight,
    gate_scale,
    up_weight,
    up_scale,
    down_weight,
    down_scale,
    gain_second,
):
    inputs = activations.astype(jnp.float32)
    features = activations.shape[1] * lax.axis_size("cb")
    gate_local = gate_weight.astype(jnp.bfloat16)
    up_local = up_weight.astype(jnp.bfloat16)
    down_local = down_weight.astype(jnp.bfloat16)
    gathered = gathered_by_axis(activations, RA, 0)
    wide_rows = gathered.astype(jnp.float32)
    row_squares = jnp.sum(wide_rows * wide_rows, axis=1)
    scaled = (wide_rows * gain_first).astype(jnp.bfloat16)
    contract = (((1,), (1,)), ((), ()))
    gate_part = lax.dot_general(gate_local, scaled, contract, preferred_element_type=jnp.float32)
    up_part = lax.dot_general(up_local, scaled, contract, preferred_element_type=jnp.float32)
    squares, gate_sum, up_sum = (
        over_copies(row_squares.astype(jnp.bfloat16), "cb").astype(jnp.float32),
        over_copies(gate_part.astype(jnp.bfloat16), "cb").astype(jnp.float32),
        over_copies(up_part.astype(jnp.bfloat16), "cb").astype(jnp.float32),
    )
    rscale_first = lax.rsqrt(squares / features + EPS)[None, :]
    gate_full = gate_sum * rscale_first * gate_scale[:, None]
    up_full = up_sum * rscale_first * up_scale[:, None]
    hidden = (jax.nn.silu(gate_full) * up_full).astype(jnp.bfloat16)
    summed = summed_on_arrival(
        lax.dot_general(
            hidden, down_local, (((0,), (0,)), ((), ())), preferred_element_type=jnp.float32
        ).astype(jnp.bfloat16),
        RA,
        0,
    )
    stream = 0.1 * inputs + summed * down_scale
    second = of_everyone(jnp.sum(stream * stream, axis=1), "cb")
    rscale_second = lax.rsqrt(second / features + EPS)[:, None]
    return (stream * rscale_second * gain_second).astype(jnp.bfloat16)


def solution(mesh):
    torus = Mesh(mesh.devices.reshape(16, 4, mesh.shape["cb"]), ("ra_0", "ra_1", "cb"))
    in_specs = (
        P(RA, "cb"),
        P("cb"),
        P(RA, "cb"),
        P(RA),
        P(RA, "cb"),
        P(RA),
        P(RA, "cb"),
        P("cb"),
        P("cb"),
    )
    out_specs = P(RA, "cb")
    return jax.shard_map(
        per_device, mesh=torus, in_specs=in_specs, out_specs=out_specs, check_vma=False
    )
```

profile of v0, /device:TPU:1, one launch (start us, length us, event | category | flops | bytes accessed | tf_op | source)
XLA Modules:
  0.0 207.7 jit_solution(14315099195980583526)
XLA Ops:
  0.0 10.5 %all-gather = bf16[4,12,512]{2,1,0:T(8,128)(2,1)S(1)} all-gather(bf16[1,12,512]{2,1,0:T(8,128)(2,1)} %bitcast.6), channel_id=1, replica_groups=mesh['ra_0'=16,'ra_1'=4,'cb'=8] {'ra_1'}, dimensions={0}, use_global_device_ids=true | all-gather | bytes 61440 | tf_op jit(solution)/shard_map/all_gather | solution.py:15
  10.5 33.2 %all_gather.7 = bf16[768,512]{1,0:T(8,128)(2,1)S(1)} all-gather(bf16[48,512]{1,0:T(8,128)(2,1)S(1)} %reshape.38), channel_id=1, replica_groups=mesh['ra_0'=16,'ra_1'=4,'cb'=8] {'ra_0'}, dimensions={0}, use_global_device_ids=true | all-gather | bytes 835584 | tf_op jit(solution)/shard_map/all_gather | solution.py:15
  43.7 0.2 fusion.1
  44.0 0.5 broadcast.45
  44.5 0.7 reduce.2
  45.2 0.6 reshape.39
  45.8 14.7 %all-to-all-start.1 = ((bf16[8,2,384]{2,1,0:T(2,128)(2,1)}), bf16[8,2,384]{2,1,0:T(2,128)(2,1)S(1)}, u32[]{:S(2)}, u32[]{:S(2)}) async-start(bf16[8,2,384]{2,1,0:T(2,128)(2,1)} %reshape.39), calls=%async_computation.1 | async-start | bytes 24576 | tf_op jit(solution)/shard_map/all_to_all | solution.py:21
  60.5 1.4 fusion.2
  62.0 3.2 %all-to-all-done.1 = bf16[8,2,384]{2,1,0:T(2,128)(2,1)S(1)} async-done(((bf16[8,2,384]{2,1,0:T(2,128)(2,1)}), bf16[8,2,384]{2,1,0:T(2,128)(2,1)S(1)}, u32[]{:S(2)}, u32[]{:S(2)}) %all-to-all-start.1) | async-done | bytes 12320 | tf_op jit(solution)/shard_map/all_to_all | solution.py:21
  65.2 1.5 broadcast_in_dim.8
  66.7 0.0 copy-start.1
  66.7 4.3 %all-to-all-start = ((bf16[8,176,768]{2,1,0:T(8,128)(2,1)}), bf16[8,176,768]{2,1,0:T(8,128)(2,1)S(1)}, u32[]{:S(2)}, u32[]{:S(2)}) async-start(bf16[8,176,768]{2,1,0:T(8,128)(2,1)} %broadcast_in_dim.8), calls=%async_computation | async-start | bytes 4325376 | tf_op jit(solution)/shard_map/all_to_all | solution.py:21
  71.0 0.0 copy-done.1
  71.0 1.4 fusion.3
  72.4 25.5 %all-to-all-done = bf16[8,176,768]{2,1,0:T(8,128)(2,1)S(1)} async-done(((bf16[8,176,768]{2,1,0:T(8,128)(2,1)}), bf16[8,176,768]{2,1,0:T(8,128)(2,1)S(1)}, u32[]{:S(2)}, u32[]{:S(2)}) %all-to-all-start) | async-done | bytes 2162720 | tf_op jit(solution)/shard_map/all_to_all | solution.py:21
  97.9 1.5 broadcast_in_dim.10
  99.4 5.2 %all-to-all-start.2 = ((bf16[8,176,768]{2,1,0:T(8,128)(2,1)}), bf16[8,176,768]{2,1,0:T(8,128)(2,1)}, u32[]{:S(2)}, u32[]{:S(2)}) async-start(bf16[8,176,768]{2,1,0:T(8,128)(2,1)} %broadcast_in_dim.10), calls=%async_computation.2 | async-start | bytes 4325376 | tf_op jit(solution)/shard_map/all_to_all | solution.py:21
  104.7 0.0 copy-start.4
  104.7 0.0 copy-start.5
  104.7 0.0 copy-start.6
  104.7 0.3 convert_reduce_fusion.1
  105.0 26.7 %all-to-all-done.2 = bf16[8,176,768]{2,1,0:T(8,128)(2,1)} async-done(((bf16[8,176,768]{2,1,0:T(8,128)(2,1)}), bf16[8,176,768]{2,1,0:T(8,128)(2,1)}, u32[]{:S(2)}, u32[]{:S(2)}) %all-to-all-start.2) | async-done | bytes 2162720 | tf_op jit(solution)/shard_map/all_to_all | solution.py:21
  131.7 2.0 convert_reduce_fusion
  133.6 0.0 copy-done.4
  133.6 0.0 copy-done.5
  133.6 0.0 copy-done.6
  133.6 0.5 convolution_convert_fusion
  134.2 0.0 copy-start
  134.2 0.0 copy-start.2
  134.2 0.0 copy-start.3
  134.2 0.2 reshape.36
  134.4 60.5 %all_to_all.27 = bf16[64,12,512]{2,1,0:T(8,128)(2,1)S(1)} all-to-all(bf16[64,12,512]{2,1,0:T(8,128)(2,1)S(1)} %reshape.36), channel_id=1, replica_groups=mesh['ra_0'=16,'ra_1'=4,'cb'=8] {'ra_0','ra_1'}, dimensions={0} | all-to-all | bytes 1572864 | tf_op jit(solution)/shard_map/all_to_all | solution.py:38
  194.8 0.2 convert_reduce_fusion.2
  195.0 0.0 copy-done
  195.0 0.0 copy-done.2
  195.1 0.1 multiply_reduce_fusion
  195.2 11.8 %all_to_all.28 = f32[8,1,12]{2,1,0:T(1,128)S(1)} all-to-all(f32[8,1,12]{2,1,0:T(1,128)S(1)} %broadcast_in_dim.11), channel_id=1, replica_groups=mesh['ra_0'=16,'ra_1'=4,'cb'=8] {'cb'}, dimensions={0} | all-to-all | bytes 768 | tf_op jit(solution)/shard_map/all_to_all | solution.py:21
  207.0 0.0 copy-done.3
  207.0 0.7 multiply_convert_fusion.2
  (8 shorter events, 0.1 us)
Async XLA Ops:
  45.8 19.4 %all-to-all-start.1 = ((bf16[8,2,384]{2,1,0:T(2,128)(2,1)}), bf16[8,2,384]{2,1,0:T(2,128)(2,1)S(1)}, u32[]{:S(2)}, u32[]{:S(2)}) async-start(bf16[8,2,384]{2,1,0:T(2,128)(2,1)} %reshape.39), calls=%async_computation.1 | async-start | bytes 24576 | tf_op jit(solution)/shard_map/all_to_all | solution.py:21
  66.7 4.3 %copy-start.1 = (f32[512]{0:T(512)S(1)}, f32[512]{0:T(512)}, u32[]{:S(2)}) copy-start(f32[512]{0:T(512)} %param.10) | copy-start | bytes 6148
  66.7 31.3 %all-to-all-start = ((bf16[8,176,768]{2,1,0:T(8,128)(2,1)}), bf16[8,176,768]{2,1,0:T(8,128)(2,1)S(1)}, u32[]{:S(2)}, u32[]{:S(2)}) async-start(bf16[8,176,768]{2,1,0:T(8,128)(2,1)} %broadcast_in_dim.8), calls=%async_computation | async-start | bytes 4325376 | tf_op jit(solution)/shard_map/all_to_all | solution.py:21
  99.4 32.2 %all-to-all-start.2 = ((bf16[8,176,768]{2,1,0:T(8,128)(2,1)}), bf16[8,176,768]{2,1,0:T(8,128)(2,1)}, u32[]{:S(2)}, u32[]{:S(2)}) async-start(bf16[8,176,768]{2,1,0:T(8,128)(2,1)} %broadcast_in_dim.10), calls=%async_computation.2 | async-start | bytes 4325376 | tf_op jit(solution)/shard_map/all_to_all | solution.py:21
  104.7 29.0 %copy-start.4 = (f32[176,512]{1,0:T(8,128)S(1)}, f32[176,512]{1,0:T(8,128)}, u32[]{:S(2)}) copy-start(f32[176,512]{1,0:T(8,128)} %param.15) | copy-start | bytes 1081348
  104.7 29.0 %copy-start.5 = (f32[176]{0:T(256)S(1)}, f32[176]{0:T(256)}, u32[]{:S(2)}) copy-start(f32[176]{0:T(256)} %param.14) | copy-start | bytes 2116
  104.7 29.0 %copy-start.6 = (f32[176]{0:T(256)S(1)}, f32[176]{0:T(256)}, u32[]{:S(2)}) copy-start(f32[176]{0:T(256)} %param.12) | copy-start | bytes 2116
  134.2 60.9 %copy-start = (bf16[12,512]{1,0:T(8,128)(2,1)S(1)}, bf16[12,512]{1,0:T(8,128)(2,1)}, u32[]{:S(2)}) copy-start(bf16[12,512]{1,0:T(8,128)(2,1)} %param.9) | copy-start | bytes 36868
  134.2 60.9 %copy-start.2 = (f32[512]{0:T(512)S(1)}, f32[512]{0:T(512)}, u32[]{:S(2)}) copy-start(f32[512]{0:T(512)} %param.16) | copy-start | bytes 6148
  134.2 72.8 %copy-start.3 = (f32[512]{0:T(512)S(1)}, f32[512]{0:T(512)}, u32[]{:S(2)}) copy-start(f32[512]{0:T(512)} %param.17) | copy-start | bytes 6148
where the time goes:
time: 208 us
  blocking collectives  116 us (56%)
  waiting for transfers between devices  55.4 us (27%)
  starting transfers between devices  24.3 us (12%)
  local copies, waits for them, and re-layouts  4.35 us (2%)
  other arithmetic  4.24 us (2%)
  matrix products  3.33 us (2%)
    all_to_all x1, blocking collectives, summed_on_arrival(): blocks = lax.all_to_all(split_up(value, dim, peers), axis, 0, 0, tiled=True)  60.5 us
    all_to_all x3, waiting for transfers between devices, from_everyone(): lax.all_to_all(jnp.broadcast_to(value[None], (peers, *value.shape)), axis...  55.4 us
    all_gather x2, blocking collectives, gathered_by_axis(): value = lax.all_gather(value, axis, axis=dim, tiled=True)  43.7 us
    all_to_all x3, starting transfers between devices, from_everyone(): lax.all_to_all(jnp.broadcast_to(value[None], (peers, *value.shape)), axis...  24.3 us
    all_to_all x1, blocking collectives, from_everyone(): lax.all_to_all(jnp.broadcast_to(value[None], (peers, *value.shape)), axis...  11.8 us
  transfers between devices with their start and end apart: 3, of which 3 were waited for; matrix products, arithmetic and copies ran while one was open for 2% of the time, Pallas kernels for 0%

commit v1 on v0

v1 whole, which is shorter than its diff:
```python
import jax
import jax.numpy as jnp
from jax import lax
from jax.sharding import Mesh
from jax.sharding import PartitionSpec as P

RA = ("zh", "zl", "y")
NEAR = ("zl", "y")
EPS = 1e-06


def from_everyone(value, axes):
    peers = lax.axis_size(axes)
    return lax.all_to_all(
        jnp.broadcast_to(value[None], (peers, *value.shape)), axes, 0, 0, tiled=True
    )


def gathered(value, axes):
    everything = from_everyone(value, axes)
    return everything.reshape(-1, *value.shape[1:])


def summed_on_arrival(value, axes):
    peers = lax.axis_size(axes)
    blocks = value.reshape(peers, -1, *value.shape[1:])
    arrived = lax.all_to_all(blocks, axes, 0, 0, tiled=True)
    return jnp.sum(arrived.astype(jnp.float32), axis=0)


def per_device(
    activations,
    gain_first,
    gate_weight,
    gate_scale,
    up_weight,
    up_scale,
    down_weight,
    down_scale,
    gain_second,
):
    bf16 = jnp.bfloat16
    units = gate_weight.shape[0]
    inputs = activations.astype(jnp.float32)
    features = activations.shape[1] * lax.axis_size("cb")
    both_local = jnp.concatenate([gate_weight, up_weight], axis=0).astype(bf16)
    down_local = down_weight.astype(bf16)

    tokens = gathered(gathered(activations, "zh"), NEAR)
    wide = tokens.astype(jnp.float32)
    squares = jnp.sum(wide * wide, axis=1, keepdims=True)
    squares_high = squares.astype(bf16)
    squares_low = (squares - squares_high.astype(jnp.float32)).astype(bf16)
    scaled = (wide * gain_first).astype(bf16)
    part = lax.dot_general(
        scaled, both_local, (((1,), (1,)), ((), ())), preferred_element_type=jnp.float32
    ).astype(bf16)
    full = summed_on_arrival(
        jnp.concatenate([part, squares_high, squares_low], axis=1), "cb"
    )
    total = full[:, 2 * units : 2 * units + 1] + full[:, 2 * units + 1 :]
    rscale_first = lax.rsqrt(total / features + EPS)
    gate = full[:, :units] * rscale_first * gate_scale
    up = full[:, units : 2 * units] * rscale_first * up_scale
    hidden = gathered((jax.nn.silu(gate) * up).astype(bf16), "cb")
    mixed = lax.dot_general(
        hidden, down_local, (((1,), (0,)), ((), ())), preferred_element_type=jnp.float32
    ).astype(bf16)
    near = summed_on_arrival(mixed, NEAR).astype(bf16)
    summed = summed_on_arrival(near, "zh")
    stream = 0.1 * inputs + summed * down_scale
    second = jnp.sum(from_everyone(jnp.sum(stream * stream, axis=1), "cb"), axis=0)
    rscale_second = lax.rsqrt(second / features + EPS)[:, None]
    return (stream * rscale_second * gain_second).astype(bf16)


def solution(mesh):
    torus = Mesh(
        mesh.devices.reshape(8, 2, 4, mesh.shape["cb"]), ("zh", "zl", "y", "cb")
    )
    in_specs = (
        P(RA, "cb"),
        P("cb"),
        P(RA, "cb"),
        P(RA),
        P(RA, "cb"),
        P(RA),
        P(RA, "cb"),
        P("cb"),
        P("cb"),
    )
    return jax.shard_map(
        per_device, mesh=torus, in_specs=in_specs, out_specs=P(RA, "cb"), check_vma=False
    )
```

time: 208 us -> 121 us (0.58)
  waiting for transfers between devices: 55.4 us -> 8.24 us
  starting transfers between devices: 24.3 us -> 5.53 us
  blocking collectives: 116 us -> 100 us
  matrix products: 3.33 us -> 0.87 us
  other arithmetic: 4.24 us -> 1.98 us
    all_to_all x3 -> x1, waiting for transfers between devices: 55.4 us -> 8.24 us  [from_everyone(): lax.all_to_all(jnp.broadcast_to(value[None], (peers, *value.shape)), axes...]
    all_gather x2 -> x0, blocking collectives: 43.7 us -> none  [gathered_by_axis(): value = lax.all_gather(value, axis, axis=dim, tiled=True)]
    all_to_all x2 -> x6, blocking collectives: 72.2 us -> 100 us  [the longest x3 50.7 us: summed_on_arrival(): arrived = lax.all_to_all(blocks, axes, 0, 0, tiled=True)]
    all_to_all x3 -> x1, starting transfers between devices: 24.3 us -> 5.53 us  [from_everyone(): lax.all_to_all(jnp.broadcast_to(value[None], (peers, *value.shape)), axes...]
    dot_general x3 -> x2, matrix products: 3.33 us -> 0.87 us  [the longest x1 0.48 us: per_device(): lax.dot_general(scaled, both_local, (((1,), (1,)), ((), ())), preferred_e...]
    reduce_sum x7 -> x6, other arithmetic: 2.84 us -> 0.61 us  [the longest x1 0.24 us: per_device(): squares = jnp.sum(wide * wide, axis=1, keepdims=True)]
  transfers between devices with their start and end apart: 3 -> 1, of which waited for: 3 -> 1; matrix products, arithmetic and copies ran while one was open for 2% -> 0% of each run, Pallas kernels for 0% -> 0%
where the time goes in v1:
time: 121 us
  blocking collectives  100 us (83%)
  waiting for transfers between devices  8.24 us (7%)
  starting transfers between devices  5.53 us (5%)
  local copies, waits for them, and re-layouts  3.58 us (3%)
  other arithmetic  1.98 us (2%)
    all_to_all x3, blocking collectives, summed_on_arrival(): arrived = lax.all_to_all(blocks, axes, 0, 0, tiled=True)  50.7 us
    all_to_all x3, blocking collectives, from_everyone(): lax.all_to_all(jnp.broadcast_to(value[None], (peers, *value.shape)), axes...  49.4 us
    all_to_all x1, waiting for transfers between devices, from_everyone(): lax.all_to_all(jnp.broadcast_to(value[None], (peers, *value.shape)), axes...  8.24 us
    all_to_all x1, starting transfers between devices, from_everyone(): lax.all_to_all(jnp.broadcast_to(value[None], (peers, *value.shape)), axes...  5.53 us
  transfers between devices with their start and end apart: 1, of which 1 were waited for; matrix products, arithmetic and copies ran while one was open for 0% of the time, Pallas kernels for 0%

profile of v1, /device:TPU:1, one launch (start us, length us, event | category | flops | bytes accessed | tf_op | source)
XLA Modules:
  0.0 120.5 jit_solution(18033898347087547807)
XLA Ops:
  0.0 0.7 broadcast_in_dim.10
  0.7 28.6 %all_to_all.36 = bf16[8,12,512]{2,1,0:T(8,128)(2,1)S(1)} all-to-all(bf16[8,12,512]{2,1,0:T(8,128)(2,1)S(1)} %broadcast_in_dim.10), channel_id=1, replica_groups=mesh['zh'=8,'zl'=2,'y'=4,'cb'=8] {'zh'}, dimensions={0} | all-to-all | bytes 196608 | tf_op jit(solution)/shard_map/all_to_all | solution.py:14
  29.4 0.9 broadcast_in_dim.12
  30.3 0.0 copy-start
  30.3 0.0 copy-start.1
  30.3 5.5 %all-to-all-start.1 = ((bf16[8,96,512]{2,1,0:T(8,128)(2,1)}), bf16[8,96,512]{2,1,0:T(8,128)(2,1)S(1)}, u32[]{:S(2)}, u32[]{:S(2)}) async-start(bf16[8,96,512]{2,1,0:T(8,128)(2,1)} %broadcast_in_dim.12), calls=%async_computation.1 | async-start | bytes 1572864 | tf_op jit(solution)/shard_map/all_to_all | solution.py:14
  35.8 0.0 copy-done
  35.9 0.0 copy-done.1
  35.9 0.0 copy-start.5
  35.9 8.2 %all-to-all-done.1 = bf16[8,96,512]{2,1,0:T(8,128)(2,1)S(1)} async-done(((bf16[8,96,512]{2,1,0:T(8,128)(2,1)}), bf16[8,96,512]{2,1,0:T(8,128)(2,1)S(1)}, u32[]{:S(2)}, u32[]{:S(2)}) %all-to-all-start.1) | async-done | bytes 786464 | tf_op jit(solution)/shard_map/all_to_all | solution.py:14
  44.2 0.2 multiply_reduce_fusion
  44.4 0.0 copy-done.5
  44.4 0.1 fusion
  44.6 0.5 convolution_convert_fusion.1
  45.1 0.3 copy.37
  45.4 0.2 copy.39
  45.6 0.2 copy.38
  45.8 0.2 pad_maximum_fusion
  46.0 0.0 copy-start.7
  46.0 0.0 copy-start.8
  46.0 19.4 %all_to_all.37 = bf16[8,96,354]{2,1,0:T(8,128)(2,1)S(1)} all-to-all(bf16[8,96,354]{2,1,0:T(8,128)(2,1)S(1)} %pad_maximum_fusion), channel_id=1, replica_groups=mesh['zh'=8,'zl'=2,'y'=4,'cb'=8] {'cb'}, dimensions={0} | all-to-all | bytes 1087488 | tf_op jit(solution)/shard_map/all_to_all | solution.py:27
  65.4 0.1 convert_reduce_fusion
  65.4 0.2 fusion.12
  65.6 0.0 copy-done.7
  65.6 0.0 copy-done.8
  65.7 0.1 fusion.7
  65.8 0.1 copy.40
  65.9 0.1 broadcast_in_dim.13
  65.9 10.9 %all_to_all.38 = bf16[8,96,176]{1,2,0:T(8,128)(2,1)S(1)} all-to-all(bf16[8,96,176]{1,2,0:T(8,128)(2,1)S(1)} %broadcast_in_dim.13), channel_id=1, replica_groups=mesh['zh'=8,'zl'=2,'y'=4,'cb'=8] {'cb'}, dimensions={0} | all-to-all | bytes 540672 | tf_op jit(solution)/shard_map/all_to_all | solution.py:14
  76.8 0.0 copy-start.2
  76.8 0.1 copy.41
  76.9 0.3 reshape.64
  77.2 0.6 copy-done.2
  77.8 0.4 convolution_convert_fusion
  78.2 14.1 %all_to_all.39 = bf16[8,96,512]{2,1,0:T(8,128)(2,1)S(1)} all-to-all(bf16[8,96,512]{2,1,0:T(8,128)(2,1)S(1)} %bitcast.17), channel_id=1, replica_groups=mesh['zh'=8,'zl'=2,'y'=4,'cb'=8] {'zl','y'}, dimensions={0} | all-to-all | bytes 1572864 | tf_op jit(solution)/shard_map/all_to_all | solution.py:27
  92.3 0.0 copy-start.3
  92.3 0.0 copy-start.4
  92.3 0.0 copy-start.6
  92.3 0.1 reduce_sum.62
  92.5 17.2 %all_to_all.40 = bf16[8,12,512]{2,1,0:T(8,128)(2,1)S(1)} all-to-all(bf16[8,12,512]{2,1,0:T(8,128)(2,1)S(1)} %reshape.66), channel_id=1, replica_groups=mesh['zh'=8,'zl'=2,'y'=4,'cb'=8] {'zh'}, dimensions={0} | all-to-all | bytes 196608 | tf_op jit(solution)/shard_map/all_to_all | solution.py:27
  109.7 0.0 copy-done.3
  109.8 0.0 copy-done.4
  109.8 0.1 multiply_reduce_fusion.1
  109.9 9.9 %all_to_all.41 = f32[8,1,12]{2,1,0:T(1,128)S(1)} all-to-all(f32[8,1,12]{2,1,0:T(1,128)S(1)} %broadcast_in_dim.14), channel_id=1, replica_groups=mesh['zh'=8,'zl'=2,'y'=4,'cb'=8] {'cb'}, dimensions={0} | all-to-all | bytes 768 | tf_op jit(solution)/shard_map/all_to_all | solution.py:14
  119.9 0.0 copy-done.6
  119.9 0.7 multiply_convert_fusion
  (9 shorter events, 0.2 us)
Async XLA Ops:
  30.3 5.5 %copy-start = (f32[176,512]{1,0:T(8,128)S(1)}, f32[176,512]{1,0:T(8,128)}, u32[]{:S(2)}) copy-start(f32[176,512]{1,0:T(8,128)} %param.11) | copy-start | bytes 1081348
  30.3 5.6 %copy-start.1 = (f32[176,512]{1,0:T(8,128)S(1)}, f32[176,512]{1,0:T(8,128)}, u32[]{:S(2)}) copy-start(f32[176,512]{1,0:T(8,128)} %param.13) | copy-start | bytes 1081348
  30.3 13.9 %all-to-all-start.1 = ((bf16[8,96,512]{2,1,0:T(8,128)(2,1)}), bf16[8,96,512]{2,1,0:T(8,128)(2,1)S(1)}, u32[]{:S(2)}, u32[]{:S(2)}) async-start(bf16[8,96,512]{2,1,0:T(8,128)(2,1)} %broadcast_in_dim.12), calls=%async_computation.1 | async-start | bytes 1572864 | tf_op jit(solution)/shard_map/all_to_all | solution.py:14
  35.9 8.5 %copy-start.5 = (f32[512]{0:T(512)S(1)}, f32[512]{0:T(512)}, u32[]{:S(2)}) copy-start(f32[512]{0:T(512)} %param.10) | copy-start | bytes 6148
  46.0 19.7 %copy-start.7 = (f32[176]{0:T(256)S(1)}, f32[176]{0:T(256)}, u32[]{:S(2)}) copy-start(f32[176]{0:T(256)} %param.14) | copy-start | bytes 2116
  46.0 19.7 %copy-start.8 = (f32[176]{0:T(256)S(1)}, f32[176]{0:T(256)}, u32[]{:S(2)}) copy-start(f32[176]{0:T(256)} %param.12) | copy-start | bytes 2116
  76.8 1.0 copy-start.2
  92.3 17.4 %copy-start.3 = (bf16[12,512]{1,0:T(8,128)(2,1)S(1)}, bf16[12,512]{1,0:T(8,128)(2,1)}, u32[]{:S(2)}) copy-start(bf16[12,512]{1,0:T(8,128)(2,1)} %param.9) | copy-start | bytes 36868
  92.3 17.4 %copy-start.4 = (f32[512]{0:T(512)S(1)}, f32[512]{0:T(512)}, u32[]{:S(2)}) copy-start(f32[512]{0:T(512)} %param.16) | copy-start | bytes 6148
  92.3 27.5 %copy-start.6 = (f32[512]{0:T(512)S(1)}, f32[512]{0:T(512)}, u32[]{:S(2)}) copy-start(f32[512]{0:T(512)} %param.17) | copy-start | bytes 6148

commit v2 on v1

v2 whole, which is shorter than its diff:
```python
import jax
import jax.numpy as jnp
from jax import lax
from jax.sharding import Mesh
from jax.sharding import PartitionSpec as P


RA = ("z", "y")
EPS = 1e-06
PAD = 32


def from_everyone(value, axes):
    peers = lax.axis_size(axes)
    return lax.all_to_all(
        jnp.broadcast_to(value[None], (peers, *value.shape)), axes, 0, 0, tiled=True
    )


def gathered(value, axes):
    everything = from_everyone(value, axes)
    return everything.reshape(-1, *value.shape[1:])


def summed_on_arrival(value, axes):
    peers = lax.axis_size(axes)
    blocks = value.reshape(peers, -1, *value.shape[1:])
    arrived = lax.all_to_all(blocks, axes, 0, 0, tiled=True)
    return jnp.sum(arrived.astype(jnp.float32), axis=0)


def moved(value, axis, distance):
    size = lax.axis_size(axis)
    pairs = [(place, (place + distance) % size) for place in range(size)]
    return lax.ppermute(value, axis, pairs)


def in_three(value):
    terms = []
    for _ in range(3):
        term = lax.reduce_precision(value, 8, 7)
        terms.append(term.astype(jnp.bfloat16))
        value = value - term
    return terms


def per_device(
    activations,
    gain_first,
    gate_weight,
    gate_scale,
    up_weight,
    up_scale,
    down_weight,
    down_scale,
    gain_second,
):
    bf16, f32 = jnp.bfloat16, jnp.float32
    units, width = gate_weight.shape
    inputs = activations.astype(f32)
    features = width * lax.axis_size("cb")

    scales = jnp.stack(in_three(jnp.concatenate([gate_scale, up_scale])))
    scales = jnp.pad(scales, ((0, PAD // 2 - 3), (0, width - 2 * units)))
    own = jnp.concatenate(
        [
            gate_weight.astype(bf16),
            up_weight.astype(bf16),
            down_weight.astype(bf16),
            scales,
        ],
        axis=0,
    )
    half = own.shape[0] // 2
    before = moved(own, "y", 1)
    after = moved(own, "y", -1)
    upper = moved(before[:half], "y", 1)
    lower = moved(after[half:], "y", -1)
    column = [own, before, after, jnp.concatenate([upper, lower], axis=0)]

    tokens = gathered(activations, "z")
    wide = tokens.astype(f32)
    squares = jnp.sum(wide * wide, axis=1, keepdims=True)
    scaled = (wide * gain_first).astype(bf16)
    squares_high = lax.reduce_precision(squares, 8, 7)
    squares_low = lax.reduce_precision(squares - squares_high, 8, 7).astype(bf16)
    squares_high = squares_high.astype(bf16)
    filler = jnp.zeros((scaled.shape[0], PAD - 2), bf16)
    parts = []
    for block in column:
        part = lax.dot_general(
            scaled,
            block[: 2 * units],
            (((1,), (1,)), ((), ())),
            preferred_element_type=f32,
        )
        parts += [part.astype(bf16), squares_high, squares_low, filler]
    full = summed_on_arrival(jnp.concatenate(parts, axis=1), "cb")
    total = full[:, 2 * units] + full[:, 2 * units + 1]
    rscale_first = lax.rsqrt(total / features + EPS)[:, None]
    hidden = []
    for index, block in enumerate(column):
        scales = block[3 * units : 3 * units + 3, : 2 * units].astype(f32)
        scales = scales[0] + scales[1] + scales[2]
        first = index * (2 * units + PAD)
        gate = full[:, first : first + units] * rscale_first * scales[:units]
        first = first + units
        up = full[:, first : first + units] * rscale_first * scales[units:]
        hidden.append((jax.nn.silu(gate) * up).astype(bf16))
    hidden = gathered(jnp.concatenate(hidden, axis=1), "cb")
    down = jnp.concatenate([block[2 * units : 3 * units] for block in column], axis=0)
    mixed = lax.dot_general(
        hidden, down, (((1,), (0,)), ((), ())), preferred_element_type=f32
    ).astype(bf16)
    summed = summed_on_arrival(mixed, "z")
    stream = 0.1 * inputs + summed * down_scale
    second = jnp.sum(from_everyone(jnp.sum(stream * stream, axis=1), "cb"), axis=0)
    rscale_second = lax.rsqrt(second / features + EPS)[:, None]
    return (stream * rscale_second * gain_second).astype(bf16)


def solution(mesh):
    torus = Mesh(mesh.devices.reshape(16, 4, mesh.shape["cb"]), ("z", "y", "cb"))
    in_specs = (
        P(RA, "cb"),
        P("cb"),
        P(RA, "cb"),
        P(RA),
        P(RA, "cb"),
        P(RA),
        P(RA, "cb"),
        P("cb"),
        P("cb"),
    )
    return jax.shard_map(
        per_device, mesh=torus, in_specs=in_specs, out_specs=P(RA, "cb"), check_vma=False
    )
```

time: 121 us -> 111 us (0.917)
  blocking collectives: 100 us -> 34.8 us
  starting transfers between devices: 5.53 us -> 43.2 us
  waiting for transfers between devices: 8.24 us -> 22.9 us
  other arithmetic: 1.98 us -> 3.53 us
    all_to_all x3 -> x1, blocking collectives: 49.4 us -> 13.6 us  [from_everyone(): lax.all_to_all(jnp.broadcast_to(value[None], (peers, *value.shape)), axes...]
    all_to_all x3 -> x1, blocking collectives: 50.7 us -> 21.1 us  [summed_on_arrival(): arrived = lax.all_to_all(blocks, axes, 0, 0, tiled=True)]
    ppermute x0 -> x4, starting transfers between devices: none -> 14 us  [moved(): return lax.ppermute(value, axis, pairs)]
    all_to_all x1 -> x2, starting transfers between devices: 5.53 us -> 19.2 us  [from_everyone(): lax.all_to_all(jnp.broadcast_to(value[None], (peers, *value.shape)), axes...]
    all_to_all x0 -> x1, starting transfers between devices: none -> 9.98 us  [summed_on_arrival(): arrived = lax.all_to_all(blocks, axes, 0, 0, tiled=True)]
    all_to_all x0 -> x1, waiting for transfers between devices: none -> 9.96 us  [summed_on_arrival(): arrived = lax.all_to_all(blocks, axes, 0, 0, tiled=True)]
    all_to_all x1 -> x2, waiting for transfers between devices: 8.24 us -> 12 us  [from_everyone(): lax.all_to_all(jnp.broadcast_to(value[None], (peers, *value.shape)), axes...]
    convert_element_type x2 -> x11, other arithmetic: 0.11 us -> 2.06 us  [the longest x1 1.01 us: per_device(): gate_weight.astype(bf16)]
  transfers between devices with their start and end apart: 1 -> 7, of which waited for: 1 -> 4; matrix products, arithmetic and copies ran while one was open for 0% -> 3% of each run, Pallas kernels for 0% -> 0%
where the time goes in v2:
time: 111 us; the launch traced here: 110 us
  starting transfers between devices  43.2 us (39%)
  blocking collectives  34.8 us (31%)
  waiting for transfers between devices  22.9 us (21%)
  local copies, waits for them, and re-layouts  4.24 us (4%)
  other arithmetic  3.53 us (3%)
  matrix products  1.51 us (1%)
    all_to_all x1, blocking collectives, summed_on_arrival(): arrived = lax.all_to_all(blocks, axes, 0, 0, tiled=True)  21.1 us
    all_to_all x2, starting transfers between devices, from_everyone(): lax.all_to_all(jnp.broadcast_to(value[None], (peers, *value.shape)), axes...  19.2 us
    ppermute x4, starting transfers between devices, moved(): return lax.ppermute(value, axis, pairs)  14 us
    all_to_all x1, blocking collectives, from_everyone(): lax.all_to_all(jnp.broadcast_to(value[None], (peers, *value.shape)), axes...  13.6 us
    all_to_all x2, waiting for transfers between devices, from_everyone(): lax.all_to_all(jnp.broadcast_to(value[None], (peers, *value.shape)), axes...  12 us
    all_to_all x1, starting transfers between devices, summed_on_arrival(): arrived = lax.all_to_all(blocks, axes, 0, 0, tiled=True)  9.98 us
    all_to_all x1, waiting for transfers between devices, summed_on_arrival(): arrived = lax.all_to_all(blocks, axes, 0, 0, tiled=True)  9.96 us
  transfers between devices with their start and end apart: 7, of which 4 were waited for; matrix products, arithmetic and copies ran while one was open for 3% of the time, Pallas kernels for 0%

profile of v2, /device:TPU:1, one launch (start us, length us, event | category | flops | bytes accessed | tf_op | source)
XLA Modules:
  0.0 110.5 jit_solution(7642677240544425864)
XLA Ops:
  0.0 0.8 reduce-precision_convert_fusion.2
  0.9 1.0 convert_element_type.138
  2.0 0.0 copy-start.3
  2.0 5.5 %collective-permute-start.1 = (bf16[544,512]{1,0:T(8,128)(2,1)S(1)}, bf16[544,512]{1,0:T(8,128)(2,1)S(1)}, u32[]{:S(2)}, u32[]{:S(2)}) collective-permute-start(bf16[544,512]{1,0:T(8,128)(2,1)S(1)} %fusion.8), channel_id=1, source_target_pairs={{0,24},{8,0},{16,8},{24,16},{1,25},{9,1},{17,9},{25,17},{2,26},{10... | collective-permute-start | bytes 1671176 | tf_op jit(solution)/shard_map/ppermute | solution.py:35
  7.5 1.9 %collective-permute-start = (bf16[544,512]{1,0:T(8,128)(2,1)S(1)}, bf16[544,512]{1,0:T(8,128)(2,1)S(1)}, u32[]{:S(2)}, u32[]{:S(2)}) collective-permute-start(bf16[544,512]{1,0:T(8,128)(2,1)S(1)} %fusion.8), channel_id=1, source_target_pairs={{0,8},{8,16},{16,24},{24,0},{1,9},{9,17},{17,25},{25,1},{2,10},{10... | collective-permute-start | bytes 1671176 | tf_op jit(solution)/shard_map/ppermute | solution.py:35
  9.4 0.0 copy-done.3
  9.4 0.7 broadcast_in_dim.8
  10.2 14.9 %all-to-all-start = ((bf16[16,12,512]{2,1,0:T(8,128)(2,1)}), bf16[16,12,512]{2,1,0:T(8,128)(2,1)S(1)}, u32[]{:S(2)}, u32[]{:S(2)}) async-start(bf16[16,12,512]{2,1,0:T(8,128)(2,1)} %broadcast_in_dim.8), calls=%async_computation | async-start | bytes 524288 | tf_op jit(solution)/shard_map/all_to_all | solution.py:15
  25.1 0.1 fusion.43
  25.2 0.0 collective-permute-done.1
  25.2 0.1 fusion.45
  25.3 4.6 %collective-permute-start.3 = (bf16[272,512]{1,0:T(8,128)(2,1)S(1)}, bf16[272,512]{1,0:T(8,128)(2,1)S(1)}, u32[]{:S(2)}, u32[]{:S(2)}) collective-permute-start(bf16[272,512]{1,0:T(8,128)(2,1)S(1)} %slice.202), channel_id=1, source_target_pairs={{0,24},{8,0},{16,8},{24,16},{1,25},{9,1},{17,9},{25,17},{2,26},{10... | collective-permute-start | bytes 835592 | tf_op jit(solution)/shard_map/ppermute | solution.py:35
  29.9 0.0 collective-permute-done
  29.9 0.7 slice.201
  30.6 2.0 %collective-permute-start.2 = (bf16[272,512]{1,0:T(8,128)(2,1)}, bf16[272,512]{1,0:T(8,128)(2,1)S(1)}, u32[]{:S(2)}, u32[]{:S(2)}) collective-permute-start(bf16[272,512]{1,0:T(8,128)(2,1)} %slice.201), channel_id=1, source_target_pairs={{0,8},{8,16},{16,24},{24,0},{1,9},{9,17},{17,25},{25,1},{2,10},{10... | collective-permute-start | bytes 835592 | tf_op jit(solution)/shard_map/ppermute | solution.py:35
  32.7 0.1 fusion.44
  32.8 5.2 %all-to-all-done = bf16[16,12,512]{2,1,0:T(8,128)(2,1)S(1)} async-done(((bf16[16,12,512]{2,1,0:T(8,128)(2,1)}), bf16[16,12,512]{2,1,0:T(8,128)(2,1)S(1)}, u32[]{:S(2)}, u32[]{:S(2)}) %all-to-all-start) | async-done | bytes 196640 | tf_op jit(solution)/shard_map/all_to_all | solution.py:15
  38.0 0.1 multiply_reduce_fusion
  38.1 0.1 reduce_sum.48
  38.3 0.3 convolution_convert_fusion.4
  38.6 0.3 convolution_convert_fusion.2
  38.9 0.1 copy.45
  39.1 0.1 copy.44
  39.2 0.3 convolution_convert_fusion.3
  39.5 0.0 collective-permute-done.3
  39.5 1.0 collective-permute-done.2
  40.5 0.3 convolution_convert_fusion.1
  40.8 1.2 %concatenate.68 = bf16[8,24,1536]{2,1,0:T(8,128)(2,1)} concatenate(bf16[8,24,352]{2,1,0:T(8,128)(2,1)S(1)} %bitcast.23, bf16[8,24,1]{2,1,0:T(8,128)(2,1)S(1)} %copy.44, bf16[8,24,1]{2,1,0:T(8,128)(2,1)S(1)} %copy.45, bf16[8,24,30]{2,1,0:T(8,128)(2,1)S(1)} %broadcast_in_dim.9, bf16[8,24,352]{2,1,0:T(8,128)(2,1)S(1)} %bitcast.25, bf16[8,24,1]{2,1,0:T(8,128)(2,1)S(1)} %copy.44, ...), dimensions={2} | concatenate | bytes 1179648 | tf_op jit(solution)/shard_map/concatenate | solution.py:98
  42.0 10.0 %all-to-all-start.1 = ((bf16[8,24,1536]{2,1,0:T(8,128)(2,1)}), bf16[8,24,1536]{2,1,0:T(8,128)(2,1)S(1)}, u32[]{:S(2)}, u32[]{:S(2)}) async-start(bf16[8,24,1536]{2,1,0:T(8,128)(2,1)} %concatenate.68), calls=%async_computation.1 | async-start | bytes 1179648 | tf_op jit(solution)/shard_map/all_to_all | solution.py:28
  52.0 0.1 fusion.46
  52.1 10.0 %all-to-all-done.1 = bf16[8,24,1536]{2,1,0:T(8,128)(2,1)S(1)} async-done(((bf16[8,24,1536]{2,1,0:T(8,128)(2,1)}), bf16[8,24,1536]{2,1,0:T(8,128)(2,1)S(1)}, u32[]{:S(2)}, u32[]{:S(2)}) %all-to-all-start.1) | async-done | bytes 589856 | tf_op jit(solution)/shard_map/all_to_all | solution.py:28
  62.0 0.1 convert_reduce_fusion
  62.1 0.2 fusion.34
  62.3 0.1 fusion.29
  62.4 0.1 pad_maximum_fusion.2
  62.5 0.7 broadcast_in_dim.10
  63.3 4.3 %all-to-all-start.2 = ((bf16[8,24,704]{2,1,0:T(8,128)(2,1)}), bf16[8,24,704]{2,1,0:T(8,128)(2,1)S(1)}, u32[]{:S(2)}, u32[]{:S(2)}) async-start(bf16[8,24,704]{2,1,0:T(8,128)(2,1)} %broadcast_in_dim.10), calls=%async_computation.2 | async-start | bytes 589824 | tf_op jit(solution)/shard_map/all_to_all | solution.py:15
  67.6 0.0 copy-done
  67.6 6.8 %all-to-all-done.2 = bf16[8,24,704]{2,1,0:T(8,128)(2,1)S(1)} async-done(((bf16[8,24,704]{2,1,0:T(8,128)(2,1)}), bf16[8,24,704]{2,1,0:T(8,128)(2,1)S(1)}, u32[]{:S(2)}, u32[]{:S(2)}) %all-to-all-start.2) | async-done | bytes 270368 | tf_op jit(solution)/shard_map/all_to_all | solution.py:15
  74.4 0.3 convolution_convert_fusion
  74.7 0.0 copy-start.4
  74.7 0.0 copy-start.6
  74.8 21.1 %all_to_all.26 = bf16[16,12,512]{2,1,0:T(8,128)(2,1)S(1)} all-to-all(bf16[16,12,512]{2,1,0:T(8,128)(2,1)S(1)} %reshape.217), channel_id=1, replica_groups=mesh['z'=16,'y'=4,'cb'=8] {'z'}, dimensions={0} | all-to-all | bytes 393216 | tf_op jit(solution)/shard_map/all_to_all | solution.py:28
  95.9 0.1 convert_reduce_fusion.1
  96.0 0.1 multiply_reduce_fusion.1
  96.1 13.6 %all_to_all.27 = f32[8,1,12]{2,1,0:T(1,128)S(1)} all-to-all(f32[8,1,12]{2,1,0:T(1,128)S(1)} %broadcast_in_dim.11), channel_id=1, replica_groups=mesh['z'=16,'y'=4,'cb'=8] {'cb'}, dimensions={0} | all-to-all | bytes 768 | tf_op jit(solution)/shard_map/all_to_all | solution.py:15
  109.8 0.0 copy-done.6
  109.8 0.7 multiply_convert_fusion.1
  (33 shorter events, 0.4 us)
Async XLA Ops:
  0.0 1.9 %copy-start.1 = (f32[176,512]{1,0:T(8,128)S(1)}, f32[176,512]{1,0:T(8,128)}, u32[]{:S(2)}) copy-start(f32[176,512]{1,0:T(8,128)} %param.13) | copy-start | bytes 1081348
  0.0 1.9 %copy-start.2 = (f32[176,512]{1,0:T(8,128)S(1)}, f32[176,512]{1,0:T(8,128)}, u32[]{:S(2)}) copy-start(f32[176,512]{1,0:T(8,128)} %param.15) | copy-start | bytes 1081348
  2.0 7.5 %copy-start.3 = (bf16[12,512]{1,0:T(8,128)(2,1)S(1)}, bf16[12,512]{1,0:T(8,128)(2,1)}, u32[]{:S(2)}) copy-start(bf16[12,512]{1,0:T(8,128)(2,1)} %param.9) | copy-start | bytes 36868
  2.0 23.1 %collective-permute-start.1 = (bf16[544,512]{1,0:T(8,128)(2,1)S(1)}, bf16[544,512]{1,0:T(8,128)(2,1)S(1)}, u32[]{:S(2)}, u32[]{:S(2)}) collective-permute-start(bf16[544,512]{1,0:T(8,128)(2,1)S(1)} %fusion.8), channel_id=1, source_target_pairs={{0,24},{8,0},{16,8},{24,16},{1,25},{9,1},{17,9},{25,17},{2,26},{10... | collective-permute-start | bytes 1671176 | tf_op jit(solution)/shard_map/ppermute | solution.py:35
  7.5 22.4 %collective-permute-start = (bf16[544,512]{1,0:T(8,128)(2,1)S(1)}, bf16[544,512]{1,0:T(8,128)(2,1)S(1)}, u32[]{:S(2)}, u32[]{:S(2)}) collective-permute-start(bf16[544,512]{1,0:T(8,128)(2,1)S(1)} %fusion.8), channel_id=1, source_target_pairs={{0,8},{8,16},{16,24},{24,0},{1,9},{9,17},{17,25},{25,1},{2,10},{10... | collective-permute-start | bytes 1671176 | tf_op jit(solution)/shard_map/ppermute | solution.py:35
  10.2 27.8 %all-to-all-start = ((bf16[16,12,512]{2,1,0:T(8,128)(2,1)}), bf16[16,12,512]{2,1,0:T(8,128)(2,1)S(1)}, u32[]{:S(2)}, u32[]{:S(2)}) async-start(bf16[16,12,512]{2,1,0:T(8,128)(2,1)} %broadcast_in_dim.8), calls=%async_computation | async-start | bytes 524288 | tf_op jit(solution)/shard_map/all_to_all | solution.py:15
  25.2 42.4 %copy-start = (bf16[544,512]{1,0:T(8,128)(2,1)}, bf16[544,512]{1,0:T(8,128)(2,1)S(1)}, u32[]{:S(2)}) copy-start(bf16[544,512]{1,0:T(8,128)(2,1)S(1)} %collective-permute-done.1) | copy-start | bytes 1671172
  25.3 14.2 %collective-permute-start.3 = (bf16[272,512]{1,0:T(8,128)(2,1)S(1)}, bf16[272,512]{1,0:T(8,128)(2,1)S(1)}, u32[]{:S(2)}, u32[]{:S(2)}) collective-permute-start(bf16[272,512]{1,0:T(8,128)(2,1)S(1)} %slice.202), channel_id=1, source_target_pairs={{0,24},{8,0},{16,8},{24,16},{1,25},{9,1},{17,9},{25,17},{2,26},{10... | collective-permute-start | bytes 835592 | tf_op jit(solution)/shard_map/ppermute | solution.py:35
  30.6 7.6 %copy-start.5 = (f32[512]{0:T(512)S(1)}, f32[512]{0:T(512)}, u32[]{:S(2)}) copy-start(f32[512]{0:T(512)} %param.10) | copy-start | bytes 6148
  30.6 9.9 %collective-permute-start.2 = (bf16[272,512]{1,0:T(8,128)(2,1)}, bf16[272,512]{1,0:T(8,128)(2,1)S(1)}, u32[]{:S(2)}, u32[]{:S(2)}) collective-permute-start(bf16[272,512]{1,0:T(8,128)(2,1)} %slice.201), channel_id=1, source_target_pairs={{0,8},{8,16},{16,24},{24,0},{1,9},{9,17},{17,25},{25,1},{2,10},{10... | collective-permute-start | bytes 835592 | tf_op jit(solution)/shard_map/ppermute | solution.py:35
  42.0 20.0 %all-to-all-start.1 = ((bf16[8,24,1536]{2,1,0:T(8,128)(2,1)}), bf16[8,24,1536]{2,1,0:T(8,128)(2,1)S(1)}, u32[]{:S(2)}, u32[]{:S(2)}) async-start(bf16[8,24,1536]{2,1,0:T(8,128)(2,1)} %concatenate.68), calls=%async_computation.1 | async-start | bytes 1179648 | tf_op jit(solution)/shard_map/all_to_all | solution.py:28
  63.3 11.1 %all-to-all-start.2 = ((bf16[8,24,704]{2,1,0:T(8,128)(2,1)}), bf16[8,24,704]{2,1,0:T(8,128)(2,1)S(1)}, u32[]{:S(2)}, u32[]{:S(2)}) async-start(bf16[8,24,704]{2,1,0:T(8,128)(2,1)} %broadcast_in_dim.10), calls=%async_computation.2 | async-start | bytes 589824 | tf_op jit(solution)/shard_map/all_to_all | solution.py:15
  67.6 6.8 %slice-start = ((bf16[544,512]{1,0:T(8,128)(2,1)}), bf16[176,512]{1,0:T(8,128)(2,1)S(1)}, s32[]{:S(2)}) async-start(bf16[544,512]{1,0:T(8,128)(2,1)} %copy-done), calls=%async_computation.5 | async-start | bytes 360448 | tf_op jit(solution)/shard_map/slice | solution.py:111
  74.7 21.3 %copy-start.4 = (f32[512]{0:T(512)S(1)}, f32[512]{0:T(512)}, u32[]{:S(2)}) copy-start(f32[512]{0:T(512)} %param.16) | copy-start | bytes 6148
  74.7 35.1 %copy-start.6 = (f32[512]{0:T(512)S(1)}, f32[512]{0:T(512)}, u32[]{:S(2)}) copy-start(f32[512]{0:T(512)} %param.17) | copy-start | bytes 6148

commit v3 on v1

v3 whole, which is shorter than its diff:
```python
import jax
import jax.numpy as jnp
from jax import lax
from jax.experimental import pallas as pl
from jax.experimental.pallas import tpu as pltpu
from jax.sharding import Mesh
from jax.sharding import PartitionSpec as P


RA = ("z", "y")
EPS = 1e-06
LANES = 128
WIDE = 384
SPLIT = 256


def whole(value):
    shape = value.shape
    return pl.BlockSpec(shape, lambda _: (0,) * len(shape))


def local(kernel, out, args, specs=None, **cost):
    return pl.pallas_call(
        kernel,
        grid=(1,),
        in_specs=specs or [whole(arg) for arg in args],
        out_specs=whole(out),
        out_shape=out,
        compiler_params=pltpu.CompilerParams(vmem_limit_bytes=16 * 2**20),
        cost_estimate=pl.CostEstimate(
            flops=cost.get("flops", 10**6),
            bytes_accessed=sum(arg.size * arg.dtype.itemsize for arg in (*args, out)),
            transcendentals=0,
        ),
    )(*args)


def pack_kernel(
    gate_hbm,
    up_hbm,
    down_hbm,
    gate_scale_hbm,
    up_scale_hbm,
    gain_first_hbm,
    gain_second_hbm,
    down_scale_hbm,
    out_ref,
    gain_first_ref,
    gain_second_ref,
    down_scale_ref,
    gate_ref,
    up_ref,
    down_ref,
    gate_scale_ref,
    up_scale_ref,
    end_ref,
    sems,
):
    bf16, f32 = jnp.bfloat16, jnp.float32
    units = gate_ref.shape[0]
    rest = units - LANES
    pairs = (
        (gate_hbm, gate_ref),
        (up_hbm, up_ref),
        (gate_scale_hbm, gate_scale_ref),
        (up_scale_hbm, up_scale_ref),
        (down_hbm, down_ref),
        (gain_first_hbm, gain_first_ref),
        (gain_second_hbm, gain_second_ref),
        (down_scale_hbm, down_scale_ref),
    )
    copies = [
        pltpu.make_async_copy(source, target, sems.at[place])
        for place, (source, target) in enumerate(pairs)
    ]
    for copy in copies:
        copy.start()
    end_ref[...] = jnp.zeros_like(end_ref)

    second = 2 * LANES
    third = second + rest
    fourth = third + rest
    copies[0].wait()
    out_ref[0:LANES] = gate_ref[0:LANES].astype(bf16)
    out_ref[second:third] = gate_ref[LANES:units].astype(bf16)
    copies[1].wait()
    out_ref[LANES:second] = up_ref[0:LANES].astype(bf16)
    out_ref[third:fourth] = up_ref[LANES:units].astype(bf16)

    copies[2].wait()
    copies[3].wait()
    end_ref[0:1, 0:rest] = gate_scale_ref[0:1, LANES:units]
    end_ref[8:9, 0:rest] = up_scale_ref[0:1, LANES:units]
    ends = end_ref[0:8] + pltpu.roll(end_ref[8:16], rest, 1)
    tiles = (gate_scale_ref[0:1, 0:LANES], up_scale_ref[0:1, 0:LANES], ends[0:1])
    row = lax.broadcasted_iota(jnp.int32, (WIDE - fourth, LANES), 0)
    for place, value in enumerate(tiles):
        high = value.astype(bf16).astype(f32)
        left = value - high
        middle = left.astype(bf16).astype(f32)
        low = left - middle
        pad = jnp.where(row == 0, high, 0.0)
        pad = jnp.where(row == 1, middle, pad)
        pad = jnp.where(row == 2, low, pad)
        out_ref[fourth:WIDE, place * LANES : (place + 1) * LANES] = pad.astype(bf16)
    out_ref[fourth:WIDE, 3 * LANES :] = jnp.zeros(
        (WIDE - fourth, out_ref.shape[1] - 3 * LANES), bf16
    )
    copies[4].wait()
    out_ref[WIDE : WIDE + units] = down_ref[...].astype(bf16)
    for copy in copies[5:]:
        copy.wait()


def part_kernel(
    token_ref, gain_ref, own_ref, before_ref, after_ref, upper_ref, lower_ref, out_ref
):
    bf16, f32 = jnp.bfloat16, jnp.float32
    wide = token_ref[...].astype(f32)
    squares = jnp.sum(wide * wide, axis=1, keepdims=True)
    high = squares.astype(bf16).astype(f32)
    low = squares - high
    scaled = (wide * gain_ref[...]).astype(bf16)

    def product(rows):
        return lax.dot_general(
            scaled, rows, (((1,), (1,)), ((), ())), preferred_element_type=f32
        )

    used = WIDE - 32
    first = product(own_ref[0:WIDE])
    place = lax.broadcasted_iota(jnp.int32, first.shape, 1)
    first = jnp.where(place == used, high, first)
    first = jnp.where(place == used + 1, low, first)
    out_ref[:, 0:WIDE] = first.astype(bf16)
    out_ref[:, WIDE : 2 * WIDE] = product(before_ref[0:WIDE]).astype(bf16)
    out_ref[:, 2 * WIDE : 3 * WIDE] = product(after_ref[0:WIDE]).astype(bf16)
    last = 3 * WIDE + SPLIT
    out_ref[:, 3 * WIDE : last] = product(upper_ref[...]).astype(bf16)
    out_ref[:, last : 4 * WIDE] = product(lower_ref[0 : WIDE - SPLIT]).astype(bf16)


def hidden_kernel(
    features, rest, part_ref, own_ref, before_ref, after_ref, lower_ref, out_ref
):
    bf16, f32 = jnp.bfloat16, jnp.float32
    peers, _, _ = out_ref.shape
    used = WIDE - 32

    def summed(first):
        total = part_ref[0, :, first : first + LANES].astype(f32)
        for peer in range(1, peers):
            total = total + part_ref[peer, :, first : first + LANES].astype(f32)
        return total

    mixed = summed(2 * LANES)
    place = lax.broadcasted_iota(jnp.int32, mixed.shape, 1)
    mark = used - 2 * LANES
    squares = jnp.where((place == mark) | (place == mark + 1), mixed, 0.0)
    squares = jnp.sum(squares, axis=1, keepdims=True)
    rscale = lax.rsqrt(squares / features + EPS)

    def store(first, value):
        for peer in range(peers):
            out_ref[peer, :, first : first + LANES] = value.astype(bf16)

    def gated(gate, up):
        return gate / (1.0 + jnp.exp(-gate)) * up

    ends = []
    for index, ref in enumerate((own_ref, before_ref, after_ref, lower_ref)):
        scales = ref[...].astype(f32)
        scales = scales[0:1] + scales[1:2] + scales[2:3]
        first = index * WIDE
        gate = summed(first) * rscale * scales[:, 0:LANES]
        up = summed(first + LANES) * rscale * scales[:, LANES : 2 * LANES]
        store(index * LANES, gated(gate, up))
        end = mixed if index == 0 else summed(first + 2 * LANES)
        end = end * rscale * scales[:, 2 * LANES : 3 * LANES]
        end = gated(end, pltpu.roll(end, LANES - rest, 1))
        ends.append(jnp.where(place < rest, end, 0.0))
    for pair in range(2):
        joined = ends[2 * pair] + pltpu.roll(ends[2 * pair + 1], LANES // 2, 1)
        store((4 + pair) * LANES, joined)


def down_kernel(
    rest, hidden_ref, own_ref, before_ref, after_ref, lower_ref, out_ref, ends_ref
):
    f32 = jnp.float32
    total = None
    ends_ref[...] = jnp.zeros_like(ends_ref)
    for index, ref in enumerate((own_ref, before_ref, after_ref, lower_ref)):
        first = WIDE - SPLIT if index == 3 else WIDE
        value = jnp.dot(
            hidden_ref[:, index * LANES : (index + 1) * LANES],
            ref[first : first + LANES],
            preferred_element_type=f32,
        )
        total = value if total is None else total + value
        start = index * (LANES // 2)
        ends_ref[start : start + rest] = ref[first + LANES : first + LANES + rest]
    total = total + jnp.dot(
        hidden_ref[:, 4 * LANES : 6 * LANES], ends_ref[...], preferred_element_type=f32
    )
    out_ref[...] = total.astype(out_ref.dtype)


def from_everyone(value, axes):
    peers = lax.axis_size(axes)
    return lax.all_to_all(
        jnp.broadcast_to(value[None], (peers, *value.shape)), axes, 0, 0, tiled=True
    )


def moved(value, axis, distance):
    size = lax.axis_size(axis)
    pairs = [(place, (place + distance) % size) for place in range(size)]
    return lax.ppermute(value, axis, pairs)


def per_device(
    activations,
    gain_first,
    gate_weight,
    gate_scale,
    up_weight,
    up_scale,
    down_weight,
    down_scale,
    gain_second,
):
    bf16, f32 = jnp.bfloat16, jnp.float32
    units, width = gate_weight.shape
    rest = units - LANES
    peers = lax.axis_size("cb")
    features = width * peers
    shape = jax.ShapeDtypeStruct

    inputs = activations.astype(f32)
    weight, scale, vector = (units, width), (1, units), pltpu.VMEM((1, width), f32)
    outs = (pltpu.VMEM((WIDE + units, width), bf16), vector, vector, vector)
    own, gain_first, gain_second, down_scale = pl.pallas_call(
        pack_kernel,
        in_specs=[pl.BlockSpec(memory_space=pltpu.MemorySpace.HBM)] * 8,
        out_specs=[pl.BlockSpec(memory_space=pltpu.MemorySpace.VMEM)] * 4,
        out_shape=outs,
        scratch_shapes=[
            *[pltpu.VMEM(weight, f32)] * 3,
            *[pltpu.VMEM(scale, f32)] * 2,
            pltpu.VMEM((16, LANES), f32),
            pltpu.SemaphoreType.DMA((8,)),
        ],
        compiler_params=pltpu.CompilerParams(vmem_limit_bytes=65000000),
        cost_estimate=pl.CostEstimate(
            flops=10**6, bytes_accessed=2**20, transcendentals=0
        ),
    )(
        gate_weight,
        up_weight,
        down_weight,
        gate_scale[None],
        up_scale[None],
        gain_first[None],
        gain_second[None],
        down_scale[None],
    )
    before = moved(own, "y", 1)
    after = moved(own, "y", -1)
    upper = moved(before[:SPLIT], "y", 1)
    lower = moved(after[SPLIT:], "y", -1)

    rows = activations.reshape(-1, 4, width)
    tokens = from_everyone(rows, "z")
    tokens = tokens.reshape(-1, width)
    count = tokens.shape[0]
    part = local(
        part_kernel,
        shape((count, 4 * WIDE), bf16),
        (tokens, gain_first, own, before, after, upper, lower),
        flops=2 * count * width * 4 * WIDE,
    )
    part = lax.all_to_all(part.reshape(peers, -1, 4 * WIDE), "cb", 0, 0, tiled=True)

    def scale_rows(first):
        return pl.BlockSpec((16, width), lambda _: (first // 16, 0))

    args = (part, own, before, after, lower)
    hidden = local(
        lambda *refs: hidden_kernel(features, rest, *refs),
        shape((peers, count // peers, 6 * LANES), bf16),
        args,
        specs=[whole(part)]
        + [scale_rows(2 * units)] * 3
        + [scale_rows(2 * units - SPLIT)],
    )
    hidden = lax.all_to_all(hidden, "cb", 0, 0, tiled=True).reshape(count, 6 * LANES)
    args = (hidden, own, before, after, lower)
    out = shape((count, width), bf16)
    mixed = pl.pallas_call(
        lambda *refs: down_kernel(rest, *refs),
        grid=(1,),
        in_specs=[whole(arg) for arg in args],
        out_specs=whole(out),
        out_shape=out,
        scratch_shapes=[pltpu.VMEM((2 * LANES, width), bf16)],
        compiler_params=pltpu.CompilerParams(vmem_limit_bytes=16 * 2**20),
        cost_estimate=pl.CostEstimate(
            flops=2 * count * width * 6 * LANES, bytes_accessed=2**20, transcendentals=0
        ),
    )(*args)
    blocks = mixed.reshape(lax.axis_size("z"), -1, 4, width)
    summed = lax.all_to_all(blocks, "z", 0, 0, tiled=True)
    summed = jnp.sum(summed.astype(f32), axis=0).reshape(-1, width)
    stream = 0.1 * inputs + summed * down_scale
    second = jnp.sum(from_everyone(jnp.sum(stream * stream, axis=1), "cb"), axis=0)
    rscale_second = lax.rsqrt(second / features + EPS)[:, None]
    return (stream * rscale_second * gain_second).astype(bf16)


def solution(mesh):
    torus = Mesh(mesh.devices.reshape(16, 4, mesh.shape["cb"]), ("z", "y", "cb"))
    in_specs = (
        P(RA, "cb"),
        P("cb"),
        P(RA, "cb"),
        P(RA),
        P(RA, "cb"),
        P(RA),
        P(RA, "cb"),
        P("cb"),
        P("cb"),
    )
    return jax.shard_map(
        per_device, mesh=torus, in_specs=in_specs, out_specs=P(RA, "cb"), check_vma=False
    )
```

time: 121 us -> 104 us (0.86)
  blocking collectives: 100 us -> 62.9 us
  starting transfers between devices: 5.53 us -> 28.8 us
  local copies, waits for them, and re-layouts: 3.58 us -> 0.92 us
  Pallas kernels: 0 us -> 2.65 us
    all_to_all x3 -> x1, blocking collectives: 49.4 us -> 11.7 us  [from_everyone(): lax.all_to_all(jnp.broadcast_to(value[None], (peers, *value.shape)), axes...]
    ppermute x0 -> x4, starting transfers between devices: none -> 13.9 us  [moved(): return lax.ppermute(value, axis, pairs)]
    all_to_all x1, starting transfers between devices: 5.53 us -> 14.9 us  [from_everyone(): lax.all_to_all(jnp.broadcast_to(value[None], (peers, *value.shape)), axes...]
    pallas_call x0 -> x4, Pallas kernels: none -> 2.65 us  [the longest x1 1.34 us: per_device(): pl.pallas_call(pack_kernel, in_specs=[pl.BlockSpec(memory_space=pltpu.Mem...]
    all_to_all x1, waiting for transfers between devices: 8.24 us -> 5.73 us  [from_everyone(): lax.all_to_all(jnp.broadcast_to(value[None], (peers, *value.shape)), axes...]
    ppermute x0 -> x4, waiting for transfers between devices: none -> 1.46 us  [moved(): return lax.ppermute(value, axis, pairs)]
  transfers between devices with their start and end apart: 1 -> 5, of which waited for: 1 -> 2; matrix products, arithmetic and copies ran while one was open for 0% -> 1% of each run, Pallas kernels for 0% -> 0%
where the time goes in v3:
time: 104 us
  blocking collectives  62.9 us (60%)
  starting transfers between devices  28.8 us (28%)
  waiting for transfers between devices  7.19 us (7%)
  Pallas kernels  2.65 us (3%)
    all_to_all x1, blocking collectives, per_device(): summed = lax.all_to_all(blocks, 'z', 0, 0, tiled=True)  22.8 us
    all_to_all x1, blocking collectives, per_device(): lax.all_to_all(part.reshape(peers, -1, 4 * WIDE), 'cb', 0, 0, tiled=True)  18 us
    all_to_all x1, starting transfers between devices, from_everyone(): lax.all_to_all(jnp.broadcast_to(value[None], (peers, *value.shape)), axes...  14.9 us
    ppermute x4, starting transfers between devices, moved(): return lax.ppermute(value, axis, pairs)  13.9 us
    all_to_all x1, blocking collectives, from_everyone(): lax.all_to_all(jnp.broadcast_to(value[None], (peers, *value.shape)), axes...  11.7 us
    all_to_all x1, blocking collectives, per_device(): lax.all_to_all(hidden, 'cb', 0, 0, tiled=True).reshape(count, 6 * LANES)  10.4 us
    all_to_all x1, waiting for transfers between devices, from_everyone(): lax.all_to_all(jnp.broadcast_to(value[None], (peers, *value.shape)), axes...  5.73 us
  transfers between devices with their start and end apart: 5, of which 2 were waited for; matrix products, arithmetic and copies ran while one was open for 1% of the time, Pallas kernels for 0%

profile of v3, /device:TPU:1, one launch (start us, length us, event | category | flops | bytes accessed | tf_op | source)
XLA Modules:
  0.0 103.6 jit_solution(11903299854811913591)
XLA Ops:
  0.0 0.0 copy-start
  0.0 1.3 %shard_map.91 = (bf16[560,512]{1,0:T(8,128)(2,1)S(1)}, f32[1,512]{1,0:T(1,128)S(1)}, f32[1,512]{1,0:T(1,128)S(1)}, f32[1,512]{1,0:T(1,128)S(1)}) custom-call(f32[176,512]{1,0:T(8,128)} %gate_hbm.1, f32[176,512]{1,0:T(8,128)} %up_hbm.1, f32[176,512]{1,0:T(8,128)} %down_hbm.1, f32[1,176]{1,0:T(1,128)} %bitcast.19, f32[1,176]{1,0:T(1,128)} %bitcast.20, ...), custom_call_target="tpu_custom_call" | custom-call | flops 1000000 | bytes 1048576 | tf_op jit(solution)/shard_map/pallas_call | solution.py:243
  1.3 5.5 %collective-permute-start.1 = (bf16[560,512]{1,0:T(8,128)(2,1)S(1)}, bf16[560,512]{1,0:T(8,128)(2,1)S(1)}, u32[]{:S(2)}, u32[]{:S(2)}) collective-permute-start(bf16[560,512]{1,0:T(8,128)(2,1)S(1)} %get-tuple-element.10.own_ref.refs_1_), channel_id=1, source_target_pairs={{0,24},{8,0},{16,8},{24,16},{1,25},{9,1},{17,9},{25,17},{2,26},{10... | collective-permute-start | bytes 1720328 | tf_op jit(solution)/shard_map/ppermute | solution.py:219
  6.8 1.9 %collective-permute-start = (bf16[560,512]{1,0:T(8,128)(2,1)S(1)}, bf16[560,512]{1,0:T(8,128)(2,1)S(1)}, u32[]{:S(2)}, u32[]{:S(2)}) collective-permute-start(bf16[560,512]{1,0:T(8,128)(2,1)S(1)} %get-tuple-element.10.own_ref.refs_1_), channel_id=1, source_target_pairs={{0,8},{8,16},{16,24},{24,0},{1,9},{9,17},{17,25},{25,1},{2,10},{10... | collective-permute-start | bytes 1720328 | tf_op jit(solution)/shard_map/ppermute | solution.py:219
  8.7 0.0 copy-done
  8.8 0.7 broadcast_in_dim.30
  9.5 14.9 %all-to-all-start = ((bf16[16,3,4,512]{3,2,1,0:T(4,128)(2,1)}), bf16[16,3,4,512]{3,2,1,0:T(4,128)(2,1)S(1)}, u32[]{:S(2)}, u32[]{:S(2)}) async-start(bf16[16,3,4,512]{3,2,1,0:T(4,128)(2,1)} %broadcast_in_dim.30), calls=%async_computation | async-start | bytes 393216 | tf_op jit(solution)/shard_map/all_to_all | solution.py:211
  24.4 0.0 collective-permute-done.1.after_ref.refs_3_
  24.5 4.6 %collective-permute-start.3 = (bf16[304,512]{1,0:T(8,128)(2,1)S(1)}, bf16[304,512]{1,0:T(8,128)(2,1)S(1)}, u32[]{:S(2)}, u32[]{:S(2)}) collective-permute-start(bf16[304,512]{1,0:T(8,128)(2,1)S(1)} %slice.9), channel_id=1, source_target_pairs={{0,24},{8,0},{16,8},{24,16},{1,25},{9,1},{17,9},{25,17},{2,26},{10... | collective-permute-start | bytes 933896 | tf_op jit(solution)/shard_map/ppermute | solution.py:219
  29.0 0.0 collective-permute-done.before_ref.refs_2_
  29.1 1.9 %collective-permute-start.2 = (bf16[256,512]{1,0:T(8,128)(2,1)S(1)}, bf16[256,512]{1,0:T(8,128)(2,1)S(1)}, u32[]{:S(2)}, u32[]{:S(2)}) collective-permute-start(bf16[256,512]{1,0:T(8,128)(2,1)S(1)} %slice.8), channel_id=1, source_target_pairs={{0,8},{8,16},{16,24},{24,0},{1,9},{9,17},{17,25},{25,1},{2,10},{10... | collective-permute-start | bytes 786440 | tf_op jit(solution)/shard_map/ppermute | solution.py:219
  31.0 5.7 %all-to-all-done = bf16[16,3,4,512]{3,2,1,0:T(4,128)(2,1)S(1)} async-done(((bf16[16,3,4,512]{3,2,1,0:T(4,128)(2,1)}), bf16[16,3,4,512]{3,2,1,0:T(4,128)(2,1)S(1)}, u32[]{:S(2)}, u32[]{:S(2)}) %all-to-all-start) | async-done | bytes 196640 | tf_op jit(solution)/shard_map/all_to_all | solution.py:211
  36.7 0.1 reshape.27.token_ref
  36.8 1.5 %collective-permute-done.2.upper_ref = bf16[256,512]{1,0:T(8,128)(2,1)S(1)} collective-permute-done((bf16[256,512]{1,0:T(8,128)(2,1)S(1)}, bf16[256,512]{1,0:T(8,128)(2,1)S(1)}, u32[]{:S(2)}, u32[]{:S(2)}) %collective-permute-start.2) | collective-permute-done | bytes 262176 | tf_op jit(solution)/shard_map/ppermute | solution.py:219
  38.3 0.0 collective-permute-done.3.lower_ref.refs_4_
  38.3 0.7 shard_map.92
  38.9 18.0 %all_to_all.26.refs_0_ = bf16[8,24,1536]{2,1,0:T(8,128)(2,1)S(1)} all-to-all(bf16[8,24,1536]{2,1,0:T(8,128)(2,1)S(1)} %bitcast.10), channel_id=1, replica_groups=mesh['z'=16,'y'=4,'cb'=8] {'cb'}, dimensions={0} | all-to-all | bytes 1179648 | tf_op jit(solution)/shard_map/all_to_all | solution.py:283
  57.0 0.2 shard_map.93
  57.2 10.4 %all_to_all.27 = bf16[8,24,768]{2,1,0:T(8,128)(2,1)S(1)} all-to-all(bf16[8,24,768]{2,1,0:T(8,128)(2,1)S(1)} %shard_map.93), channel_id=1, replica_groups=mesh['z'=16,'y'=4,'cb'=8] {'cb'}, dimensions={0} | all-to-all | bytes 589824 | tf_op jit(solution)/shard_map/all_to_all | solution.py:297
  67.6 0.4 shard_map.94
  68.0 0.1 reshape.30
  68.1 22.8 %all_to_all.28 = bf16[16,3,4,512]{3,2,1,0:T(4,128)(2,1)S(1)} all-to-all(bf16[16,3,4,512]{3,2,1,0:T(4,128)(2,1)S(1)} %reshape.30), channel_id=1, replica_groups=mesh['z'=16,'y'=4,'cb'=8] {'z'}, dimensions={0} | all-to-all | bytes 393216 | tf_op jit(solution)/shard_map/all_to_all | solution.py:313
  90.9 0.1 convert_reduce_fusion
  91.0 0.1 multiply_reduce_fusion
  91.1 11.7 %all_to_all.29 = f32[8,1,12]{2,1,0:T(1,128)S(1)} all-to-all(f32[8,1,12]{2,1,0:T(1,128)S(1)} %broadcast_in_dim.36), channel_id=1, replica_groups=mesh['z'=16,'y'=4,'cb'=8] {'cb'}, dimensions={0} | all-to-all | bytes 768 | tf_op jit(solution)/shard_map/all_to_all | solution.py:211
  102.9 0.7 multiply_convert_fusion
  (7 shorter events, 0.1 us)
Async XLA Ops:
  0.0 8.7 %copy-start = (bf16[12,512]{1,0:T(8,128)(2,1)S(1)}, bf16[12,512]{1,0:T(8,128)(2,1)}, u32[]{:S(2)}) copy-start(bf16[12,512]{1,0:T(8,128)(2,1)} %param.9) | copy-start | bytes 36868
  1.3 23.1 %collective-permute-start.1 = (bf16[560,512]{1,0:T(8,128)(2,1)S(1)}, bf16[560,512]{1,0:T(8,128)(2,1)S(1)}, u32[]{:S(2)}, u32[]{:S(2)}) collective-permute-start(bf16[560,512]{1,0:T(8,128)(2,1)S(1)} %get-tuple-element.10.own_ref.refs_1_), channel_id=1, source_target_pairs={{0,24},{8,0},{16,8},{24,16},{1,25},{9,1},{17,9},{25,17},{2,26},{10... | collective-permute-start | bytes 1720328 | tf_op jit(solution)/shard_map/ppermute | solution.py:219
  6.8 22.2 %collective-permute-start = (bf16[560,512]{1,0:T(8,128)(2,1)S(1)}, bf16[560,512]{1,0:T(8,128)(2,1)S(1)}, u32[]{:S(2)}, u32[]{:S(2)}) collective-permute-start(bf16[560,512]{1,0:T(8,128)(2,1)S(1)} %get-tuple-element.10.own_ref.refs_1_), channel_id=1, source_target_pairs={{0,8},{8,16},{16,24},{24,0},{1,9},{9,17},{17,25},{25,1},{2,10},{10... | collective-permute-start | bytes 1720328 | tf_op jit(solution)/shard_map/ppermute | solution.py:219
  9.5 27.2 %all-to-all-start = ((bf16[16,3,4,512]{3,2,1,0:T(4,128)(2,1)}), bf16[16,3,4,512]{3,2,1,0:T(4,128)(2,1)S(1)}, u32[]{:S(2)}, u32[]{:S(2)}) async-start(bf16[16,3,4,512]{3,2,1,0:T(4,128)(2,1)} %broadcast_in_dim.30), calls=%async_computation | async-start | bytes 393216 | tf_op jit(solution)/shard_map/all_to_all | solution.py:211
  24.5 13.8 %collective-permute-start.3 = (bf16[304,512]{1,0:T(8,128)(2,1)S(1)}, bf16[304,512]{1,0:T(8,128)(2,1)S(1)}, u32[]{:S(2)}, u32[]{:S(2)}) collective-permute-start(bf16[304,512]{1,0:T(8,128)(2,1)S(1)} %slice.9), channel_id=1, source_target_pairs={{0,24},{8,0},{16,8},{24,16},{1,25},{9,1},{17,9},{25,17},{2,26},{10... | collective-permute-start | bytes 933896 | tf_op jit(solution)/shard_map/ppermute | solution.py:219
  29.1 9.2 %collective-permute-start.2 = (bf16[256,512]{1,0:T(8,128)(2,1)S(1)}, bf16[256,512]{1,0:T(8,128)(2,1)S(1)}, u32[]{:S(2)}, u32[]{:S(2)}) collective-permute-start(bf16[256,512]{1,0:T(8,128)(2,1)S(1)} %slice.8), channel_id=1, source_target_pairs={{0,8},{8,16},{16,24},{24,0},{1,9},{9,17},{17,25},{25,1},{2,10},{10... | collective-permute-start | bytes 786440 | tf_op jit(solution)/shard_map/ppermute | solution.py:219

commit v4 on v3

--- a/solution.py
+++ b/solution.py
@@ -10,8 +10,10 @@
 RA = ("z", "y")
 EPS = 1e-06
 LANES = 128
+USED = 352
+DOWN = 368
 WIDE = 384
-SPLIT = 256
+SPLIT = 224
 
 
 def whole(value):
@@ -19,16 +21,17 @@
     return pl.BlockSpec(shape, lambda _: (0,) * len(shape))
 
 
-def local(kernel, out, args, specs=None, **cost):
+def local(kernel, out, args, specs=None, scratch=(), flops=10**6):
     return pl.pallas_call(
         kernel,
         grid=(1,),
         in_specs=specs or [whole(arg) for arg in args],
         out_specs=whole(out),
         out_shape=out,
+        scratch_shapes=scratch,
         compiler_params=pltpu.CompilerParams(vmem_limit_bytes=16 * 2**20),
         cost_estimate=pl.CostEstimate(
-            flops=cost.get("flops", 10**6),
+            flops=flops,
             bytes_accessed=sum(arg.size * arg.dtype.itemsize for arg in (*args, out)),
             transcendentals=0,
         ),
@@ -44,22 +47,27 @@
     gain_first_hbm,
     gain_second_hbm,
     down_scale_hbm,
+    rows_hbm,
     out_ref,
     gain_first_ref,
     gain_second_ref,
     down_scale_ref,
+    rows_ref,
+    sent_hbm,
     gate_ref,
     up_ref,
     down_ref,
     gate_scale_ref,
     up_scale_ref,
     end_ref,
+    block_ref,
     sems,
 ):
     bf16, f32 = jnp.bfloat16, jnp.float32
     units = gate_ref.shape[0]
     rest = units - LANES
     pairs = (
+        (rows_hbm, rows_ref),
         (gate_hbm, gate_ref),
         (up_hbm, up_ref),
         (gate_scale_hbm, gate_scale_ref),
@@ -81,19 +89,30 @@
     third = second + rest
     fourth = third + rest
     copies[0].wait()
+    rows = rows_ref[...].astype(f32)
+    blocks, size, _ = block_ref.shape
+    for block in range(blocks):
+        block_ref[block] = rows[block * size : (block + 1) * size].astype(bf16)
+    sends = [
+        pltpu.make_async_copy(block_ref, sent_hbm.at[peer], sems.at[len(copies) + peer])
+        for peer in range(sent_hbm.shape[0])
+    ]
+    for send in sends:
+        send.start()
+    copies[1].wait()
     out_ref[0:LANES] = gate_ref[0:LANES].astype(bf16)
     out_ref[second:third] = gate_ref[LANES:units].astype(bf16)
-    copies[1].wait()
+    copies[2].wait()
     out_ref[LANES:second] = up_ref[0:LANES].astype(bf16)
     out_ref[third:fourth] = up_ref[LANES:units].astype(bf16)
 
-    copies[2].wait()
     copies[3].wait()
+    copies[4].wait()
     end_ref[0:1, 0:rest] = gate_scale_ref[0:1, LANES:units]
     end_ref[8:9, 0:rest] = up_scale_ref[0:1, LANES:units]
     ends = end_ref[0:8] + pltpu.roll(end_ref[8:16], rest, 1)
     tiles = (gate_scale_ref[0:1, 0:LANES], up_scale_ref[0:1, 0:LANES], ends[0:1])
-    row = lax.broadcasted_iota(jnp.int32, (WIDE - fourth, LANES), 0)
+    row = lax.broadcasted_iota(jnp.int32, (DOWN - fourth, LANES), 0)
     for place, value in enumerate(tiles):
         high = value.astype(bf16).astype(f32)
         left = value - high
@@ -102,18 +121,26 @@
         pad = jnp.where(row == 0, high, 0.0)
         pad = jnp.where(row == 1, middle, pad)
         pad = jnp.where(row == 2, low, pad)
-        out_ref[fourth:WIDE, place * LANES : (place + 1) * LANES] = pad.astype(bf16)
-    out_ref[fourth:WIDE, 3 * LANES :] = jnp.zeros(
-        (WIDE - fourth, out_ref.shape[1] - 3 * LANES), bf16
-    )
-    copies[4].wait()
-    out_ref[WIDE : WIDE + units] = down_ref[...].astype(bf16)
-    for copy in copies[5:]:
+        out_ref[fourth:DOWN, place * LANES : (place + 1) * LANES] = pad.astype(bf16)
+    out_ref[fourth:DOWN, 3 * LANES :] = jnp.zeros(
+        (DOWN - fourth, out_ref.shape[1] - 3 * LANES), bf16
+    )
+    copies[5].wait()
+    out_ref[DOWN : DOWN + units] = down_ref[...].astype(bf16)
+    for copy in copies[6:] + sends:
         copy.wait()
 
 
 def part_kernel(
-    token_ref, gain_ref, own_ref, before_ref, after_ref, upper_ref, lower_ref, out_ref
+    token_ref,
+    gain_ref,
+    own_ref,
+    before_ref,
+    after_ref,
+    upper_ref,
+    lower_ref,
+    out_ref,
+    far_ref,
 ):
     bf16, f32 = jnp.bfloat16, jnp.float32
     wide = token_ref[...].astype(f32)
@@ -127,17 +154,16 @@
             scaled, rows, (((1,), (1,)), ((), ())), preferred_element_type=f32
         )
 
-    used = WIDE - 32
+    far_ref[0:SPLIT] = upper_ref[...]
+    far_ref[SPLIT:WIDE] = lower_ref[0 : WIDE - SPLIT]
     first = product(own_ref[0:WIDE])
     place = lax.broadcasted_iota(jnp.int32, first.shape, 1)
-    first = jnp.where(place == used, high, first)
-    first = jnp.where(place == used + 1, low, first)
+    first = jnp.where(place == USED, high, first)
+    first = jnp.where(place == USED + 1, low, first)
     out_ref[:, 0:WIDE] = first.astype(bf16)
     out_ref[:, WIDE : 2 * WIDE] = product(before_ref[0:WIDE]).astype(bf16)
     out_ref[:, 2 * WIDE : 3 * WIDE] = product(after_ref[0:WIDE]).astype(bf16)
-    last = 3 * WIDE + SPLIT
-    out_ref[:, 3 * WIDE : last] = product(upper_ref[...]).astype(bf16)
-    out_ref[:, last : 4 * WIDE] = product(lower_ref[0 : WIDE - SPLIT]).astype(bf16)
+    out_ref[:, 3 * WIDE : 4 * WIDE] = product(far_ref[...]).astype(bf16)
 
 
 def hidden_kernel(
@@ -145,7 +171,6 @@
 ):
     bf16, f32 = jnp.bfloat16, jnp.float32
     peers, _, _ = out_ref.shape
-    used = WIDE - 32
 
     def summed(first):
         total = part_ref[0, :, first : first + LANES].astype(f32)
@@ -155,7 +180,7 @@
 
     mixed = summed(2 * LANES)
     place = lax.broadcasted_iota(jnp.int32, mixed.shape, 1)
-    mark = used - 2 * LANES
+    mark = USED - 2 * LANES
     squares = jnp.where((place == mark) | (place == mark + 1), mixed, 0.0)
     squares = jnp.sum(squares, axis=1, keepdims=True)
     rscale = lax.rsqrt(squares / features + EPS)
@@ -191,7 +216,7 @@
     total = None
     ends_ref[...] = jnp.zeros_like(ends_ref)
     for index, ref in enumerate((own_ref, before_ref, after_ref, lower_ref)):
-        first = WIDE - SPLIT if index == 3 else WIDE
+        first = DOWN - SPLIT if index == 3 else DOWN
         value = jnp.dot(
             hidden_ref[:, index * LANES : (index + 1) * LANES],
             ref[first : first + LANES],
@@ -237,19 +262,25 @@
     features = width * peers
     shape = jax.ShapeDtypeStruct
 
-    inputs = activations.astype(f32)
     weight, scale, vector = (units, width), (1, units), pltpu.VMEM((1, width), f32)
-    outs = (pltpu.VMEM((WIDE + units, width), bf16), vector, vector, vector)
-    own, gain_first, gain_second, down_scale = pl.pallas_call(
+    columns = lax.axis_size("z")
+    block = (activations.shape[0] // 4, 4, width)
+    sent = shape((columns, *block), bf16)
+    own = pltpu.VMEM((DOWN + units, width), bf16)
+    rows = pltpu.VMEM(activations.shape, bf16)
+    outs = (own, vector, vector, vector, rows, sent)
+    own, gain_first, gain_second, down_scale, rows, sent = pl.pallas_call(
         pack_kernel,
-        in_specs=[pl.BlockSpec(memory_space=pltpu.MemorySpace.HBM)] * 8,
-        out_specs=[pl.BlockSpec(memory_space=pltpu.MemorySpace.VMEM)] * 4,
+        in_specs=[pl.BlockSpec(memory_space=pltpu.MemorySpace.HBM)] * 9,
+        out_specs=[pl.BlockSpec(memory_space=pltpu.MemorySpace.VMEM)] * 5
+        + [pl.BlockSpec(memory_space=pltpu.MemorySpace.HBM)],
         out_shape=outs,
         scratch_shapes=[
             *[pltpu.VMEM(weight, f32)] * 3,
             *[pltpu.VMEM(scale, f32)] * 2,
             pltpu.VMEM((16, LANES), f32),
-            pltpu.SemaphoreType.DMA((8,)),
+            pltpu.VMEM(block, bf16),
+            pltpu.SemaphoreType.DMA((9 + columns,)),
         ],
         compiler_params=pltpu.CompilerParams(vmem_limit_bytes=65000000),
         cost_estimate=pl.CostEstimate(
@@ -264,20 +295,21 @@
         gain_first[None],
         gain_second[None],
         down_scale[None],
+        activations,
     )
     before = moved(own, "y", 1)
     after = moved(own, "y", -1)
     upper = moved(before[:SPLIT], "y", 1)
     lower = moved(after[SPLIT:], "y", -1)
 
-    rows = activations.reshape(-1, 4, width)
-    tokens = from_everyone(rows, "z")
+    tokens = lax.all_to_all(sent, "z", 0, 0, tiled=True)
     tokens = tokens.reshape(-1, width)
     count = tokens.shape[0]
     part = local(
         part_kernel,
         shape((count, 4 * WIDE), bf16),
         (tokens, gain_first, own, before, after, upper, lower),
+        scratch=[pltpu.VMEM((WIDE, width), bf16)],
         flops=2 * count * width * 4 * WIDE,
     )
     part = lax.all_to_all(part.reshape(peers, -1, 4 * WIDE), "cb", 0, 0, tiled=True)
@@ -295,24 +327,17 @@
         + [scale_rows(2 * units - SPLIT)],
     )
     hidden = lax.all_to_all(hidden, "cb", 0, 0, tiled=True).reshape(count, 6 * LANES)
-    args = (hidden, own, before, after, lower)
-    out = shape((count, width), bf16)
-    mixed = pl.pallas_call(
+    mixed = local(
         lambda *refs: down_kernel(rest, *refs),
-        grid=(1,),
-        in_specs=[whole(arg) for arg in args],
-        out_specs=whole(out),
-        out_shape=out,
-        scratch_shapes=[pltpu.VMEM((2 * LANES, width), bf16)],
-        compiler_params=pltpu.CompilerParams(vmem_limit_bytes=16 * 2**20),
-        cost_estimate=pl.CostEstimate(
-            flops=2 * count * width * 6 * LANES, bytes_accessed=2**20, transcendentals=0
-        ),
-    )(*args)
-    blocks = mixed.reshape(lax.axis_size("z"), -1, 4, width)
+        shape((count, width), bf16),
+        (hidden, own, before, after, lower),
+        scratch=[pltpu.VMEM((2 * LANES, width), bf16)],
+        flops=2 * count * width * 6 * LANES,
+    )
+    blocks = mixed.reshape(columns, -1, 4, width)
     summed = lax.all_to_all(blocks, "z", 0, 0, tiled=True)
     summed = jnp.sum(summed.astype(f32), axis=0).reshape(-1, width)
-    stream = 0.1 * inputs + summed * down_scale
+    stream = 0.1 * rows.astype(f32) + summed * down_scale
     second = jnp.sum(from_everyone(jnp.sum(stream * stream, axis=1), "cb"), axis=0)
     rscale_second = lax.rsqrt(second / features + EPS)[:, None]
     return (stream * rscale_second * gain_second).astype(bf16)

time: 104 us -> 103 us (level)
  transfers between devices with their start and end apart: 5 -> 5, of which waited for: 2 -> 2; matrix products, arithmetic and copies ran while one was open for 1% -> 0% of each run, Pallas kernels for 0% -> 0%
where the time goes in v4:
time: 103 us; the launch traced here: 102 us
  blocking collectives  63 us (61%)
  starting transfers between devices  28.8 us (28%)
  waiting for transfers between devices  6.49 us (6%)
  Pallas kernels  2.93 us (3%)
    all_to_all x1, blocking collectives, per_device(): summed = lax.all_to_all(blocks, 'z', 0, 0, tiled=True)  22.2 us
    all_to_all x1, blocking collectives, per_device(): lax.all_to_all(part.reshape(peers, -1, 4 * WIDE), 'cb', 0, 0, tiled=True)  18.7 us
    all_to_all x1, starting transfers between devices, per_device(): tokens = lax.all_to_all(sent, 'z', 0, 0, tiled=True)  14.9 us
    ppermute x4, starting transfers between devices, moved(): return lax.ppermute(value, axis, pairs)  13.9 us
    all_to_all x1, blocking collectives, from_everyone(): lax.all_to_all(jnp.broadcast_to(value[None], (peers, *value.shape)), axes...  11.7 us
    all_to_all x1, blocking collectives, per_device(): lax.all_to_all(hidden, 'cb', 0, 0, tiled=True).reshape(count, 6 * LANES)  10.4 us
    all_to_all x1, waiting for transfers between devices, per_device(): tokens = lax.all_to_all(sent, 'z', 0, 0, tiled=True)  5.73 us
  transfers between devices with their start and end apart: 5, of which 2 were waited for; matrix products, arithmetic and copies ran while one was open for 0% of the time, Pallas kernels for 0%

profile of v4, /device:TPU:1, one launch (start us, length us, event | category | flops | bytes accessed | tf_op | source)
XLA Modules:
  0.0 102.5 jit_solution(10612713053109190782)
XLA Ops:
  0.0 1.6 %shard_map.91 = (bf16[544,512]{1,0:T(8,128)(2,1)S(1)}, f32[1,512]{1,0:T(1,128)S(1)}, f32[1,512]{1,0:T(1,128)S(1)}, f32[1,512]{1,0:T(1,128)S(1)}, bf16[12,512]{1,...) custom-call(f32[176,512]{1,0:T(8,128)} %gate_hbm.1, f32[176,512]{1,0:T(8,128)} %up_hbm.1, f32[176,512]{1,0:T(8,128)} %down_hbm.1, ...), custom_call_target="tpu_custom_call" | custom-call | flops 1000000 | bytes 1048576 | tf_op jit(solution)/shard_map/pallas_call | solution.py:272
  1.6 5.5 %collective-permute-start.1 = (bf16[544,512]{1,0:T(8,128)(2,1)S(1)}, bf16[544,512]{1,0:T(8,128)(2,1)S(1)}, u32[]{:S(2)}, u32[]{:S(2)}) collective-permute-start(bf16[544,512]{1,0:T(8,128)(2,1)S(1)} %get-tuple-element.14.own_ref.refs_1_), channel_id=1, source_target_pairs={{0,24},{8,0},{16,8},{24,16},{1,25},{9,1},{17,9},{25,17},{2,26},{10... | collective-permute-start | bytes 1671176 | tf_op jit(solution)/shard_map/ppermute | solution.py:244
  7.1 1.9 %collective-permute-start = (bf16[544,512]{1,0:T(8,128)(2,1)S(1)}, bf16[544,512]{1,0:T(8,128)(2,1)S(1)}, u32[]{:S(2)}, u32[]{:S(2)}) collective-permute-start(bf16[544,512]{1,0:T(8,128)(2,1)S(1)} %get-tuple-element.14.own_ref.refs_1_), channel_id=1, source_target_pairs={{0,8},{8,16},{16,24},{24,0},{1,9},{9,17},{17,25},{25,1},{2,10},{10... | collective-permute-start | bytes 1671176 | tf_op jit(solution)/shard_map/ppermute | solution.py:244
  9.0 14.9 %all-to-all-start = ((bf16[16,3,4,512]{3,2,1,0:T(4,128)(2,1)}), bf16[16,3,4,512]{3,2,1,0:T(4,128)(2,1)S(1)}, u32[]{:S(2)}, u32[]{:S(2)}) async-start(bf16[16,3,4,512]{3,2,1,0:T(4,128)(2,1)} %get-tuple-element.12), calls=%async_computation | async-start | bytes 393216 | tf_op jit(solution)/shard_map/all_to_all | solution.py:305
  24.0 0.0 collective-permute-done.1.after_ref.refs_3_
  24.0 4.6 %collective-permute-start.3 = (bf16[320,512]{1,0:T(8,128)(2,1)S(1)}, bf16[320,512]{1,0:T(8,128)(2,1)S(1)}, u32[]{:S(2)}, u32[]{:S(2)}) collective-permute-start(bf16[320,512]{1,0:T(8,128)(2,1)S(1)} %slice.9), channel_id=1, source_target_pairs={{0,24},{8,0},{16,8},{24,16},{1,25},{9,1},{17,9},{25,17},{2,26},{10... | collective-permute-start | bytes 983048 | tf_op jit(solution)/shard_map/ppermute | solution.py:244
  28.6 0.0 collective-permute-done.before_ref.refs_2_
  28.6 1.9 %collective-permute-start.2 = (bf16[224,512]{1,0:T(8,128)(2,1)S(1)}, bf16[224,512]{1,0:T(8,128)(2,1)S(1)}, u32[]{:S(2)}, u32[]{:S(2)}) collective-permute-start(bf16[224,512]{1,0:T(8,128)(2,1)S(1)} %slice.8), channel_id=1, source_target_pairs={{0,8},{8,16},{16,24},{24,0},{1,9},{9,17},{17,25},{25,1},{2,10},{10... | collective-permute-start | bytes 688136 | tf_op jit(solution)/shard_map/ppermute | solution.py:244
  30.5 5.7 %all-to-all-done = bf16[16,3,4,512]{3,2,1,0:T(4,128)(2,1)S(1)} async-done(((bf16[16,3,4,512]{3,2,1,0:T(4,128)(2,1)}), bf16[16,3,4,512]{3,2,1,0:T(4,128)(2,1)S(1)}, u32[]{:S(2)}, u32[]{:S(2)}) %all-to-all-start) | async-done | bytes 196640 | tf_op jit(solution)/shard_map/all_to_all | solution.py:305
  36.3 0.1 reshape.26.token_ref
  36.3 0.8 collective-permute-done.2.upper_ref
  37.1 0.0 collective-permute-done.3.lower_ref.refs_4_
  37.1 0.7 shard_map.92
  37.8 18.7 %all_to_all.26.refs_0_ = bf16[8,24,1536]{2,1,0:T(8,128)(2,1)S(1)} all-to-all(bf16[8,24,1536]{2,1,0:T(8,128)(2,1)S(1)} %bitcast.10), channel_id=1, replica_groups=mesh['z'=16,'y'=4,'cb'=8] {'cb'}, dimensions={0} | all-to-all | bytes 1179648 | tf_op jit(solution)/shard_map/all_to_all | solution.py:315
  56.5 0.2 shard_map.93
  56.8 10.4 %all_to_all.27 = bf16[8,24,768]{2,1,0:T(8,128)(2,1)S(1)} all-to-all(bf16[8,24,768]{2,1,0:T(8,128)(2,1)S(1)} %shard_map.93), channel_id=1, replica_groups=mesh['z'=16,'y'=4,'cb'=8] {'cb'}, dimensions={0} | all-to-all | bytes 589824 | tf_op jit(solution)/shard_map/all_to_all | solution.py:329
  67.2 0.4 shard_map.94
  67.6 0.1 reshape.29
  67.6 22.2 %all_to_all.28 = bf16[16,3,4,512]{3,2,1,0:T(4,128)(2,1)S(1)} all-to-all(bf16[16,3,4,512]{3,2,1,0:T(4,128)(2,1)S(1)} %reshape.29), channel_id=1, replica_groups=mesh['z'=16,'y'=4,'cb'=8] {'z'}, dimensions={0} | all-to-all | bytes 393216 | tf_op jit(solution)/shard_map/all_to_all | solution.py:338
  89.8 0.1 convert_reduce_fusion
  89.9 0.1 multiply_reduce_fusion
  90.0 11.7 %all_to_all.29 = f32[8,1,12]{2,1,0:T(1,128)S(1)} all-to-all(f32[8,1,12]{2,1,0:T(1,128)S(1)} %broadcast_in_dim.27), channel_id=1, replica_groups=mesh['z'=16,'y'=4,'cb'=8] {'cb'}, dimensions={0} | all-to-all | bytes 768 | tf_op jit(solution)/shard_map/all_to_all | solution.py:236
  101.8 0.7 multiply_convert_fusion
  (6 shorter events, 0.1 us)
Async XLA Ops:
  1.6 22.3 %collective-permute-start.1 = (bf16[544,512]{1,0:T(8,128)(2,1)S(1)}, bf16[544,512]{1,0:T(8,128)(2,1)S(1)}, u32[]{:S(2)}, u32[]{:S(2)}) collective-permute-start(bf16[544,512]{1,0:T(8,128)(2,1)S(1)} %get-tuple-element.14.own_ref.refs_1_), channel_id=1, source_target_pairs={{0,24},{8,0},{16,8},{24,16},{1,25},{9,1},{17,9},{25,17},{2,26},{10... | collective-permute-start | bytes 1671176 | tf_op jit(solution)/shard_map/ppermute | solution.py:244
  7.1 21.5 %collective-permute-start = (bf16[544,512]{1,0:T(8,128)(2,1)S(1)}, bf16[544,512]{1,0:T(8,128)(2,1)S(1)}, u32[]{:S(2)}, u32[]{:S(2)}) collective-permute-start(bf16[544,512]{1,0:T(8,128)(2,1)S(1)} %get-tuple-element.14.own_ref.refs_1_), channel_id=1, source_target_pairs={{0,8},{8,16},{16,24},{24,0},{1,9},{9,17},{17,25},{25,1},{2,10},{10... | collective-permute-start | bytes 1671176 | tf_op jit(solution)/shard_map/ppermute | solution.py:244
  9.0 27.3 %all-to-all-start = ((bf16[16,3,4,512]{3,2,1,0:T(4,128)(2,1)}), bf16[16,3,4,512]{3,2,1,0:T(4,128)(2,1)S(1)}, u32[]{:S(2)}, u32[]{:S(2)}) async-start(bf16[16,3,4,512]{3,2,1,0:T(4,128)(2,1)} %get-tuple-element.12), calls=%async_computation | async-start | bytes 393216 | tf_op jit(solution)/shard_map/all_to_all | solution.py:305
  24.0 13.1 %collective-permute-start.3 = (bf16[320,512]{1,0:T(8,128)(2,1)S(1)}, bf16[320,512]{1,0:T(8,128)(2,1)S(1)}, u32[]{:S(2)}, u32[]{:S(2)}) collective-permute-start(bf16[320,512]{1,0:T(8,128)(2,1)S(1)} %slice.9), channel_id=1, source_target_pairs={{0,24},{8,0},{16,8},{24,16},{1,25},{9,1},{17,9},{25,17},{2,26},{10... | collective-permute-start | bytes 983048 | tf_op jit(solution)/shard_map/ppermute | solution.py:244
  28.6 8.5 %collective-permute-start.2 = (bf16[224,512]{1,0:T(8,128)(2,1)S(1)}, bf16[224,512]{1,0:T(8,128)(2,1)S(1)}, u32[]{:S(2)}, u32[]{:S(2)}) collective-permute-start(bf16[224,512]{1,0:T(8,128)(2,1)S(1)} %slice.8), channel_id=1, source_target_pairs={{0,8},{8,16},{16,24},{24,0},{1,9},{9,17},{17,25},{25,1},{2,10},{10... | collective-permute-start | bytes 688136 | tf_op jit(solution)/shard_map/ppermute | solution.py:244

commit v5 on v4

--- a/solution.py
+++ b/solution.py
@@ -9,11 +9,14 @@
 
 RA = ("z", "y")
 EPS = 1e-06
+GATHER = [[*range(10, 16), *range(10)]]
+SUM = [[*range(10, 16), *range(10)]]
+NEAR = [[*range(5, 8), *range(5)]]
 LANES = 128
 USED = 352
 DOWN = 368
 WIDE = 384
-SPLIT = 224
+SPLIT = 160
 
 
 def whole(value):
@@ -229,13 +232,6 @@
         hidden_ref[:, 4 * LANES : 6 * LANES], ends_ref[...], preferred_element_type=f32
     )
     out_ref[...] = total.astype(out_ref.dtype)
-
-
-def from_everyone(value, axes):
-    peers = lax.axis_size(axes)
-    return lax.all_to_all(
-        jnp.broadcast_to(value[None], (peers, *value.shape)), axes, 0, 0, tiled=True
-    )
 
 
 def moved(value, axis, distance):
@@ -302,7 +298,7 @@
     upper = moved(before[:SPLIT], "y", 1)
     lower = moved(after[SPLIT:], "y", -1)
 
-    tokens = lax.all_to_all(sent, "z", 0, 0, tiled=True)
+    tokens = lax.all_to_all(sent, "z", 0, 0, tiled=True, axis_index_groups=GATHER)
     tokens = tokens.reshape(-1, width)
     count = tokens.shape[0]
     part = local(
@@ -312,7 +308,8 @@
         scratch=[pltpu.VMEM((WIDE, width), bf16)],
         flops=2 * count * width * 4 * WIDE,
     )
-    part = lax.all_to_all(part.reshape(peers, -1, 4 * WIDE), "cb", 0, 0, tiled=True)
+    part = part.reshape(peers, -1, 4 * WIDE)
+    part = lax.all_to_all(part, "cb", 0, 0, tiled=True, axis_index_groups=NEAR)
 
     def scale_rows(first):
         return pl.BlockSpec((16, width), lambda _: (first // 16, 0))
@@ -326,7 +323,8 @@
         + [scale_rows(2 * units)] * 3
         + [scale_rows(2 * units - SPLIT)],
     )
-    hidden = lax.all_to_all(hidden, "cb", 0, 0, tiled=True).reshape(count, 6 * LANES)
+    hidden = lax.all_to_all(hidden, "cb", 0, 0, tiled=True, axis_index_groups=NEAR)
+    hidden = hidden.reshape(count, 6 * LANES)
     mixed = local(
         lambda *refs: down_kernel(rest, *refs),
         shape((count, width), bf16),
@@ -335,10 +333,13 @@
         flops=2 * count * width * 6 * LANES,
     )
     blocks = mixed.reshape(columns, -1, 4, width)
-    summed = lax.all_to_all(blocks, "z", 0, 0, tiled=True)
+    summed = lax.all_to_all(blocks, "z", 0, 0, tiled=True, axis_index_groups=SUM)
     summed = jnp.sum(summed.astype(f32), axis=0).reshape(-1, width)
     stream = 0.1 * rows.astype(f32) + summed * down_scale
-    second = jnp.sum(from_everyone(jnp.sum(stream * stream, axis=1), "cb"), axis=0)
+    second = jnp.sum(stream * stream, axis=1)
+    second = jnp.broadcast_to(second, (peers, *second.shape))
+    second = lax.all_to_all(second, "cb", 0, 0, tiled=True, axis_index_groups=NEAR)
+    second = jnp.sum(second, axis=0)
     rscale_second = lax.rsqrt(second / features + EPS)[:, None]
     return (stream * rscale_second * gain_second).astype(bf16)
 

time: 103 us -> 105 us (1.019)
  waiting for transfers between devices: 6.49 us -> 14.5 us
  blocking collectives: 63 us -> 55.4 us
  starting transfers between devices: 28.8 us -> 30.4 us
    ppermute x4, waiting for transfers between devices: 0.76 us -> 14.5 us  [moved(): return lax.ppermute(value, axis, pairs)]
    all_to_all x4, blocking collectives: 63 us -> 55.4 us  [the longest x1 21.6 us: per_device(): lax.all_to_all(blocks, 'z', 0, 0, tiled=True, axis_index_groups=SUM)]
    all_to_all x1, waiting for transfers between devices: 5.73 us -> 0.01 us  [per_device(): lax.all_to_all(sent, 'z', 0, 0, tiled=True, axis_index_groups=GATHER)]
    all_to_all x1, starting transfers between devices: 14.9 us -> 16.5 us  [per_device(): lax.all_to_all(sent, 'z', 0, 0, tiled=True, axis_index_groups=GATHER)]
where the time goes in v5:
time: 105 us; the launch traced here: 104 us
  blocking collectives  55.4 us (53%)
  starting transfers between devices  30.4 us (29%)
  waiting for transfers between devices  14.5 us (14%)
  Pallas kernels  2.94 us (3%)
    all_to_all x1, blocking collectives, per_device(): lax.all_to_all(blocks, 'z', 0, 0, tiled=True, axis_index_groups=SUM)  21.6 us
    all_to_all x1, starting transfers between devices, per_device(): lax.all_to_all(sent, 'z', 0, 0, tiled=True, axis_index_groups=GATHER)  16.5 us
    all_to_all x1, blocking collectives, per_device(): part = lax.all_to_all(part, 'cb', 0, 0, tiled=True, axis_index_groups=NEAR)  15.7 us
    ppermute x4, waiting for transfers between devices, moved(): return lax.ppermute(value, axis, pairs)  14.5 us
    ppermute x4, starting transfers between devices, moved(): return lax.ppermute(value, axis, pairs)  13.9 us
    all_to_all x1, blocking collectives, per_device(): lax.all_to_all(hidden, 'cb', 0, 0, tiled=True, axis_index_groups=NEAR)  9.8 us
    all_to_all x1, blocking collectives, per_device(): lax.all_to_all(second, 'cb', 0, 0, tiled=True, axis_index_groups=NEAR)  8.41 us
  transfers between devices with their start and end apart: 5, of which 2 were waited for; matrix products, arithmetic and copies ran while one was open for 0% of the time, Pallas kernels for 0%

profile of v5, /device:TPU:1, one launch (start us, length us, event | category | flops | bytes accessed | tf_op | source)
XLA Modules:
  0.0 104.5 jit_solution(11418097112201259832)
XLA Ops:
  0.0 1.6 %shard_map.91 = (bf16[544,512]{1,0:T(8,128)(2,1)S(1)}, f32[1,512]{1,0:T(1,128)S(1)}, f32[1,512]{1,0:T(1,128)S(1)}, f32[1,512]{1,0:T(1,128)S(1)}, bf16[12,512]{1,...) custom-call(f32[176,512]{1,0:T(8,128)} %gate_hbm.1, f32[176,512]{1,0:T(8,128)} %up_hbm.1, f32[176,512]{1,0:T(8,128)} %down_hbm.1, ...), custom_call_target="tpu_custom_call" | custom-call | flops 1000000 | bytes 1048576 | tf_op jit(solution)/shard_map/pallas_call | solution.py:268
  1.6 5.5 %collective-permute-start.1 = (bf16[544,512]{1,0:T(8,128)(2,1)S(1)}, bf16[544,512]{1,0:T(8,128)(2,1)S(1)}, u32[]{:S(2)}, u32[]{:S(2)}) collective-permute-start(bf16[544,512]{1,0:T(8,128)(2,1)S(1)} %get-tuple-element.14.own_ref.refs_1_), channel_id=1, source_target_pairs={{0,24},{8,0},{16,8},{24,16},{1,25},{9,1},{17,9},{25,17},{2,26},{10... | collective-permute-start | bytes 1671176 | tf_op jit(solution)/shard_map/ppermute | solution.py:240
  7.1 16.5 %all-to-all-start = ((bf16[16,3,4,512]{3,2,1,0:T(4,128)(2,1)}), bf16[16,3,4,512]{3,2,1,0:T(4,128)(2,1)S(1)}, u32[]{:S(2)}, u32[]{:S(2)}) async-start(bf16[16,3,4,512]{3,2,1,0:T(4,128)(2,1)} %get-tuple-element.12), calls=%async_computation | async-start | bytes 393216 | tf_op jit(solution)/shard_map/all_to_all | solution.py:301
  23.6 1.9 %collective-permute-start = (bf16[544,512]{1,0:T(8,128)(2,1)S(1)}, bf16[544,512]{1,0:T(8,128)(2,1)S(1)}, u32[]{:S(2)}, u32[]{:S(2)}) collective-permute-start(bf16[544,512]{1,0:T(8,128)(2,1)S(1)} %get-tuple-element.14.own_ref.refs_1_), channel_id=1, source_target_pairs={{0,8},{8,16},{16,24},{24,0},{1,9},{9,17},{17,25},{25,1},{2,10},{10... | collective-permute-start | bytes 1671176 | tf_op jit(solution)/shard_map/ppermute | solution.py:240
  25.5 0.0 collective-permute-done.1.after_ref.refs_3_
  25.6 4.6 %collective-permute-start.3 = (bf16[384,512]{1,0:T(8,128)(2,1)S(1)}, bf16[384,512]{1,0:T(8,128)(2,1)S(1)}, u32[]{:S(2)}, u32[]{:S(2)}) collective-permute-start(bf16[384,512]{1,0:T(8,128)(2,1)S(1)} %slice.9), channel_id=1, source_target_pairs={{0,24},{8,0},{16,8},{24,16},{1,25},{9,1},{17,9},{25,17},{2,26},{10... | collective-permute-start | bytes 1179656 | tf_op jit(solution)/shard_map/ppermute | solution.py:240
  30.1 9.2 %collective-permute-done.before_ref.refs_2_ = bf16[544,512]{1,0:T(8,128)(2,1)S(1)} collective-permute-done((bf16[544,512]{1,0:T(8,128)(2,1)S(1)}, bf16[544,512]{1,0:T(8,128)(2,1)S(1)}, u32[]{:S(2)}, u32[]{:S(2)}) %collective-permute-start) | collective-permute-done | bytes 557088 | tf_op jit(solution)/shard_map/ppermute | solution.py:240
  39.4 1.9 %collective-permute-start.2 = (bf16[160,512]{1,0:T(8,128)(2,1)S(1)}, bf16[160,512]{1,0:T(8,128)(2,1)S(1)}, u32[]{:S(2)}, u32[]{:S(2)}) collective-permute-start(bf16[160,512]{1,0:T(8,128)(2,1)S(1)} %slice.8), channel_id=1, source_target_pairs={{0,8},{8,16},{16,24},{24,0},{1,9},{9,17},{17,25},{25,1},{2,10},{10... | collective-permute-start | bytes 491528 | tf_op jit(solution)/shard_map/ppermute | solution.py:240
  41.3 0.0 all-to-all-done
  41.3 0.1 reshape.24.token_ref
  41.4 5.3 %collective-permute-done.2.upper_ref = bf16[160,512]{1,0:T(8,128)(2,1)S(1)} collective-permute-done((bf16[160,512]{1,0:T(8,128)(2,1)S(1)}, bf16[160,512]{1,0:T(8,128)(2,1)S(1)}, u32[]{:S(2)}, u32[]{:S(2)}) %collective-permute-start.2) | collective-permute-done | bytes 163872 | tf_op jit(solution)/shard_map/ppermute | solution.py:240
  46.6 0.0 collective-permute-done.3.lower_ref.refs_4_
  46.7 0.7 shard_map.92
  47.3 15.7 %all_to_all.26.refs_0_ = bf16[8,24,1536]{2,1,0:T(8,128)(2,1)S(1)} all-to-all(bf16[8,24,1536]{2,1,0:T(8,128)(2,1)S(1)} %bitcast.10), channel_id=1, replica_groups={{5,6,7,0,1,2,3,4},{13,14,15,8,9,10,11,12},{21,22,23,16,17,18,19,20},{29..., dimensions={0} | all-to-all | bytes 1179648 | tf_op jit(solution)/shard_map/all_to_all | solution.py:312
  63.0 0.2 shard_map.93
  63.2 9.8 %all_to_all.27 = bf16[8,24,768]{2,1,0:T(8,128)(2,1)S(1)} all-to-all(bf16[8,24,768]{2,1,0:T(8,128)(2,1)S(1)} %shard_map.93), channel_id=1, replica_groups={{5,6,7,0,1,2,3,4},{13,14,15,8,9,10,11,12},{21,22,23,16,17,18,19,20},{29..., dimensions={0} | all-to-all | bytes 589824 | tf_op jit(solution)/shard_map/all_to_all | solution.py:326
  73.0 0.4 shard_map.94
  73.4 0.1 reshape.27
  73.5 21.6 %all_to_all.28 = bf16[16,3,4,512]{3,2,1,0:T(4,128)(2,1)S(1)} all-to-all(bf16[16,3,4,512]{3,2,1,0:T(4,128)(2,1)S(1)} %reshape.27), channel_id=1, replica_groups={{320,352,384,416,448,480,0,32,64,96,128,160,192,224,256,288},{321,353,3..., dimensions={0} | all-to-all | bytes 393216 | tf_op jit(solution)/shard_map/all_to_all | solution.py:336
  95.1 0.1 convert_reduce_fusion
  95.2 0.1 multiply_reduce_fusion
  95.3 8.4 %all_to_all.29 = f32[8,1,12]{2,1,0:T(1,128)S(1)} all-to-all(f32[8,1,12]{2,1,0:T(1,128)S(1)} %broadcast_in_dim.24), channel_id=1, replica_groups={{5,6,7,0,1,2,3,4},{13,14,15,8,9,10,11,12},{21,22,23,16,17,18,19,20},{29..., dimensions={0} | all-to-all | bytes 768 | tf_op jit(solution)/shard_map/all_to_all | solution.py:341
  103.8 0.7 multiply_convert_fusion
  (6 shorter events, 0.1 us)
Async XLA Ops:
  1.6 23.9 %collective-permute-start.1 = (bf16[544,512]{1,0:T(8,128)(2,1)S(1)}, bf16[544,512]{1,0:T(8,128)(2,1)S(1)}, u32[]{:S(2)}, u32[]{:S(2)}) collective-permute-start(bf16[544,512]{1,0:T(8,128)(2,1)S(1)} %get-tuple-element.14.own_ref.refs_1_), channel_id=1, source_target_pairs={{0,24},{8,0},{16,8},{24,16},{1,25},{9,1},{17,9},{25,17},{2,26},{10... | collective-permute-start | bytes 1671176 | tf_op jit(solution)/shard_map/ppermute | solution.py:240
  7.1 34.2 %all-to-all-start = ((bf16[16,3,4,512]{3,2,1,0:T(4,128)(2,1)}), bf16[16,3,4,512]{3,2,1,0:T(4,128)(2,1)S(1)}, u32[]{:S(2)}, u32[]{:S(2)}) async-start(bf16[16,3,4,512]{3,2,1,0:T(4,128)(2,1)} %get-tuple-element.12), calls=%async_computation | async-start | bytes 393216 | tf_op jit(solution)/shard_map/all_to_all | solution.py:301
  23.6 15.8 %collective-permute-start = (bf16[544,512]{1,0:T(8,128)(2,1)S(1)}, bf16[544,512]{1,0:T(8,128)(2,1)S(1)}, u32[]{:S(2)}, u32[]{:S(2)}) collective-permute-start(bf16[544,512]{1,0:T(8,128)(2,1)S(1)} %get-tuple-element.14.own_ref.refs_1_), channel_id=1, source_target_pairs={{0,8},{8,16},{16,24},{24,0},{1,9},{9,17},{17,25},{25,1},{2,10},{10... | collective-permute-start | bytes 1671176 | tf_op jit(solution)/shard_map/ppermute | solution.py:240
  25.6 21.1 %collective-permute-start.3 = (bf16[384,512]{1,0:T(8,128)(2,1)S(1)}, bf16[384,512]{1,0:T(8,128)(2,1)S(1)}, u32[]{:S(2)}, u32[]{:S(2)}) collective-permute-start(bf16[384,512]{1,0:T(8,128)(2,1)S(1)} %slice.9), channel_id=1, source_target_pairs={{0,24},{8,0},{16,8},{24,16},{1,25},{9,1},{17,9},{25,17},{2,26},{10... | collective-permute-start | bytes 1179656 | tf_op jit(solution)/shard_map/ppermute | solution.py:240
  39.4 7.3 %collective-permute-start.2 = (bf16[160,512]{1,0:T(8,128)(2,1)S(1)}, bf16[160,512]{1,0:T(8,128)(2,1)S(1)}, u32[]{:S(2)}, u32[]{:S(2)}) collective-permute-start(bf16[160,512]{1,0:T(8,128)(2,1)S(1)} %slice.8), channel_id=1, source_target_pairs={{0,8},{8,16},{16,24},{24,0},{1,9},{9,17},{17,25},{25,1},{2,10},{10... | collective-permute-start | bytes 491528 | tf_op jit(solution)/shard_map/ppermute | solution.py:240

commit v6 on v5

--- a/solution.py
+++ b/solution.py
@@ -11,12 +11,14 @@
 EPS = 1e-06
 GATHER = [[*range(10, 16), *range(10)]]
 SUM = [[*range(10, 16), *range(10)]]
+FIRST = [(0, 1), (1, 0), (2, 3), (3, 2)]
+SECOND = [(1, 2), (2, 1), (3, 0), (0, 3)]
 NEAR = [[*range(5, 8), *range(5)]]
 LANES = 128
 USED = 352
 DOWN = 368
 WIDE = 384
-SPLIT = 160
+SPLIT = 240
 
 
 def whole(value):
@@ -232,12 +234,6 @@
         hidden_ref[:, 4 * LANES : 6 * LANES], ends_ref[...], preferred_element_type=f32
     )
     out_ref[...] = total.astype(out_ref.dtype)
-
-
-def moved(value, axis, distance):
-    size = lax.axis_size(axis)
-    pairs = [(place, (place + distance) % size) for place in range(size)]
-    return lax.ppermute(value, axis, pairs)
 
 
 def per_device(
@@ -293,10 +289,10 @@
         down_scale[None],
         activations,
     )
-    before = moved(own, "y", 1)
-    after = moved(own, "y", -1)
-    upper = moved(before[:SPLIT], "y", 1)
-    lower = moved(after[SPLIT:], "y", -1)
+    before = lax.ppermute(own, "y", FIRST)
+    after = lax.ppermute(own, "y", SECOND)
+    lower = lax.ppermute(before[SPLIT:], "y", SECOND)
+    upper = lax.ppermute(after[:SPLIT], "y", FIRST)
 
     tokens = lax.all_to_all(sent, "z", 0, 0, tiled=True, axis_index_groups=GATHER)
     tokens = tokens.reshape(-1, width)

time: 105 us -> 93.8 us (0.89)
  waiting for transfers between devices: 14.5 us -> 5.52 us
  starting transfers between devices: 30.4 us -> 28.9 us
    ppermute x4, waiting for transfers between devices: 14.5 us -> 0.62 us  [the longest x1 0.44 us: per_device(): upper = lax.ppermute(after[:SPLIT], 'y', FIRST)]
    all_to_all x1, waiting for transfers between devices: 0.01 us -> 4.9 us  [per_device(): lax.all_to_all(sent, 'z', 0, 0, tiled=True, axis_index_groups=GATHER)]
    ppermute x4, starting transfers between devices: 13.9 us -> 12.4 us  [the longest x1 4.02 us: per_device(): before = lax.ppermute(own, 'y', FIRST)]
  transfers between devices with their start and end apart: 5 -> 5, of which waited for: 2 -> 3; matrix products, arithmetic and copies ran while one was open for 0% -> 0% of each run, Pallas kernels for 0% -> 0%
where the time goes in v6:
time: 93.8 us; the launch traced here: 93.3 us
  blocking collectives  54.7 us (58%)
  starting transfers between devices  28.9 us (31%)
  waiting for transfers between devices  5.52 us (6%)
  Pallas kernels  2.93 us (3%)
    all_to_all x1, blocking collectives, per_device(): lax.all_to_all(blocks, 'z', 0, 0, tiled=True, axis_index_groups=SUM)  21.6 us
    all_to_all x1, starting transfers between devices, per_device(): lax.all_to_all(sent, 'z', 0, 0, tiled=True, axis_index_groups=GATHER)  16.5 us
    all_to_all x1, blocking collectives, per_device(): part = lax.all_to_all(part, 'cb', 0, 0, tiled=True, axis_index_groups=NEAR)  14.9 us
    all_to_all x1, blocking collectives, per_device(): lax.all_to_all(hidden, 'cb', 0, 0, tiled=True, axis_index_groups=NEAR)  9.8 us
    all_to_all x1, blocking collectives, per_device(): lax.all_to_all(second, 'cb', 0, 0, tiled=True, axis_index_groups=NEAR)  8.41 us
    all_to_all x1, waiting for transfers between devices, per_device(): lax.all_to_all(sent, 'z', 0, 0, tiled=True, axis_index_groups=GATHER)  4.9 us
    ppermute x1, starting transfers between devices, per_device(): before = lax.ppermute(own, 'y', FIRST)  4.02 us
    ppermute x1, starting transfers between devices, per_device(): after = lax.ppermute(own, 'y', SECOND)  3.81 us
  transfers between devices with their start and end apart: 5, of which 3 were waited for; matrix products, arithmetic and copies ran while one was open for 0% of the time, Pallas kernels for 0%

profile of v6, /device:TPU:1, one launch (start us, length us, event | category | flops | bytes accessed | tf_op | source)
XLA Modules:
  0.0 93.3 jit_solution(13300296804049402644)
XLA Ops:
  0.0 1.6 %shard_map.91 = (bf16[544,512]{1,0:T(8,128)(2,1)S(1)}, f32[1,512]{1,0:T(1,128)S(1)}, f32[1,512]{1,0:T(1,128)S(1)}, f32[1,512]{1,0:T(1,128)S(1)}, bf16[12,512]{1,...) custom-call(f32[176,512]{1,0:T(8,128)} %gate_hbm.1, f32[176,512]{1,0:T(8,128)} %up_hbm.1, f32[176,512]{1,0:T(8,128)} %down_hbm.1, ...), custom_call_target="tpu_custom_call" | custom-call | flops 1000000 | bytes 1048576 | tf_op jit(solution)/shard_map/pallas_call | solution.py:264
  1.6 4.0 %collective-permute-start = (bf16[544,512]{1,0:T(8,128)(2,1)S(1)}, bf16[544,512]{1,0:T(8,128)(2,1)S(1)}, u32[]{:S(2)}, u32[]{:S(2)}) collective-permute-start(bf16[544,512]{1,0:T(8,128)(2,1)S(1)} %get-tuple-element.14.own_ref.refs_1_), channel_id=1, source_target_pairs={{0,8},{8,0},{16,24},{24,16},{1,9},{9,1},{17,25},{25,17},{2,10},{10... | collective-permute-start | bytes 1671176 | tf_op jit(solution)/shard_map/ppermute | solution.py:292
  5.7 3.8 %collective-permute-start.1 = (bf16[544,512]{1,0:T(8,128)(2,1)S(1)}, bf16[544,512]{1,0:T(8,128)(2,1)S(1)}, u32[]{:S(2)}, u32[]{:S(2)}) collective-permute-start(bf16[544,512]{1,0:T(8,128)(2,1)S(1)} %get-tuple-element.14.own_ref.refs_1_), channel_id=1, source_target_pairs={{8,16},{16,8},{24,0},{0,24},{9,17},{17,9},{25,1},{1,25},{10,18},{1... | collective-permute-start | bytes 1671176 | tf_op jit(solution)/shard_map/ppermute | solution.py:293
  9.5 16.5 %all-to-all-start = ((bf16[16,3,4,512]{3,2,1,0:T(4,128)(2,1)}), bf16[16,3,4,512]{3,2,1,0:T(4,128)(2,1)S(1)}, u32[]{:S(2)}, u32[]{:S(2)}) async-start(bf16[16,3,4,512]{3,2,1,0:T(4,128)(2,1)} %get-tuple-element.12), calls=%async_computation | async-start | bytes 393216 | tf_op jit(solution)/shard_map/all_to_all | solution.py:297
  26.0 0.0 collective-permute-done.before_ref.refs_2_
  26.0 2.7 %collective-permute-start.3 = (bf16[304,512]{1,0:T(8,128)(2,1)S(1)}, bf16[304,512]{1,0:T(8,128)(2,1)S(1)}, u32[]{:S(2)}, u32[]{:S(2)}) collective-permute-start(bf16[304,512]{1,0:T(8,128)(2,1)S(1)} %slice.9), channel_id=1, source_target_pairs={{8,16},{16,8},{24,0},{0,24},{9,17},{17,9},{25,1},{1,25},{10,18},{1... | collective-permute-start | bytes 933896 | tf_op jit(solution)/shard_map/ppermute | solution.py:294
  28.7 0.0 collective-permute-done.1.after_ref.refs_3_
  28.7 1.9 %collective-permute-start.2 = (bf16[240,512]{1,0:T(8,128)(2,1)S(1)}, bf16[240,512]{1,0:T(8,128)(2,1)S(1)}, u32[]{:S(2)}, u32[]{:S(2)}) collective-permute-start(bf16[240,512]{1,0:T(8,128)(2,1)S(1)} %slice.8), channel_id=1, source_target_pairs={{0,8},{8,0},{16,24},{24,16},{1,9},{9,1},{17,25},{25,17},{2,10},{10... | collective-permute-start | bytes 737288 | tf_op jit(solution)/shard_map/ppermute | solution.py:295
  30.7 4.9 %all-to-all-done = bf16[16,3,4,512]{3,2,1,0:T(4,128)(2,1)S(1)} async-done(((bf16[16,3,4,512]{3,2,1,0:T(4,128)(2,1)}), bf16[16,3,4,512]{3,2,1,0:T(4,128)(2,1)S(1)}, u32[]{:S(2)}, u32[]{:S(2)}) %all-to-all-start) | async-done | bytes 196640 | tf_op jit(solution)/shard_map/all_to_all | solution.py:297
  35.6 0.1 reshape.24.token_ref
  35.6 0.4 collective-permute-done.2.upper_ref
  36.1 0.2 collective-permute-done.3.lower_ref.refs_4_
  36.2 0.7 shard_map.92
  36.9 14.9 %all_to_all.26.refs_0_ = bf16[8,24,1536]{2,1,0:T(8,128)(2,1)S(1)} all-to-all(bf16[8,24,1536]{2,1,0:T(8,128)(2,1)S(1)} %bitcast.10), channel_id=1, replica_groups={{5,6,7,0,1,2,3,4},{13,14,15,8,9,10,11,12},{21,22,23,16,17,18,19,20},{29..., dimensions={0} | all-to-all | bytes 1179648 | tf_op jit(solution)/shard_map/all_to_all | solution.py:308
  51.8 0.2 shard_map.93
  52.1 9.8 %all_to_all.27 = bf16[8,24,768]{2,1,0:T(8,128)(2,1)S(1)} all-to-all(bf16[8,24,768]{2,1,0:T(8,128)(2,1)S(1)} %shard_map.93), channel_id=1, replica_groups={{5,6,7,0,1,2,3,4},{13,14,15,8,9,10,11,12},{21,22,23,16,17,18,19,20},{29..., dimensions={0} | all-to-all | bytes 589824 | tf_op jit(solution)/shard_map/all_to_all | solution.py:322
  61.9 0.4 shard_map.94
  62.3 0.1 reshape.27
  62.3 21.6 %all_to_all.28 = bf16[16,3,4,512]{3,2,1,0:T(4,128)(2,1)S(1)} all-to-all(bf16[16,3,4,512]{3,2,1,0:T(4,128)(2,1)S(1)} %reshape.27), channel_id=1, replica_groups={{320,352,384,416,448,480,0,32,64,96,128,160,192,224,256,288},{321,353,3..., dimensions={0} | all-to-all | bytes 393216 | tf_op jit(solution)/shard_map/all_to_all | solution.py:332
  83.9 0.1 convert_reduce_fusion
  84.0 0.1 multiply_reduce_fusion
  84.2 8.4 %all_to_all.29 = f32[8,1,12]{2,1,0:T(1,128)S(1)} all-to-all(f32[8,1,12]{2,1,0:T(1,128)S(1)} %broadcast_in_dim.24), channel_id=1, replica_groups={{5,6,7,0,1,2,3,4},{13,14,15,8,9,10,11,12},{21,22,23,16,17,18,19,20},{29..., dimensions={0} | all-to-all | bytes 768 | tf_op jit(solution)/shard_map/all_to_all | solution.py:337
  92.6 0.7 multiply_convert_fusion
  (6 shorter events, 0.1 us)
Async XLA Ops:
  1.6 24.4 %collective-permute-start = (bf16[544,512]{1,0:T(8,128)(2,1)S(1)}, bf16[544,512]{1,0:T(8,128)(2,1)S(1)}, u32[]{:S(2)}, u32[]{:S(2)}) collective-permute-start(bf16[544,512]{1,0:T(8,128)(2,1)S(1)} %get-tuple-element.14.own_ref.refs_1_), channel_id=1, source_target_pairs={{0,8},{8,0},{16,24},{24,16},{1,9},{9,1},{17,25},{25,17},{2,10},{10... | collective-permute-start | bytes 1671176 | tf_op jit(solution)/shard_map/ppermute | solution.py:292
  5.7 23.1 %collective-permute-start.1 = (bf16[544,512]{1,0:T(8,128)(2,1)S(1)}, bf16[544,512]{1,0:T(8,128)(2,1)S(1)}, u32[]{:S(2)}, u32[]{:S(2)}) collective-permute-start(bf16[544,512]{1,0:T(8,128)(2,1)S(1)} %get-tuple-element.14.own_ref.refs_1_), channel_id=1, source_target_pairs={{8,16},{16,8},{24,0},{0,24},{9,17},{17,9},{25,1},{1,25},{10,18},{1... | collective-permute-start | bytes 1671176 | tf_op jit(solution)/shard_map/ppermute | solution.py:293
  9.5 26.1 %all-to-all-start = ((bf16[16,3,4,512]{3,2,1,0:T(4,128)(2,1)}), bf16[16,3,4,512]{3,2,1,0:T(4,128)(2,1)S(1)}, u32[]{:S(2)}, u32[]{:S(2)}) async-start(bf16[16,3,4,512]{3,2,1,0:T(4,128)(2,1)} %get-tuple-element.12), calls=%async_computation | async-start | bytes 393216 | tf_op jit(solution)/shard_map/all_to_all | solution.py:297
  26.0 10.2 %collective-permute-start.3 = (bf16[304,512]{1,0:T(8,128)(2,1)S(1)}, bf16[304,512]{1,0:T(8,128)(2,1)S(1)}, u32[]{:S(2)}, u32[]{:S(2)}) collective-permute-start(bf16[304,512]{1,0:T(8,128)(2,1)S(1)} %slice.9), channel_id=1, source_target_pairs={{8,16},{16,8},{24,0},{0,24},{9,17},{17,9},{25,1},{1,25},{10,18},{1... | collective-permute-start | bytes 933896 | tf_op jit(solution)/shard_map/ppermute | solution.py:294
  28.7 7.3 %collective-permute-start.2 = (bf16[240,512]{1,0:T(8,128)(2,1)S(1)}, bf16[240,512]{1,0:T(8,128)(2,1)S(1)}, u32[]{:S(2)}, u32[]{:S(2)}) collective-permute-start(bf16[240,512]{1,0:T(8,128)(2,1)S(1)} %slice.8), channel_id=1, source_target_pairs={{0,8},{8,0},{16,24},{24,16},{1,9},{9,1},{17,25},{25,17},{2,10},{10... | collective-permute-start | bytes 737288 | tf_op jit(solution)/shard_map/ppermute | solution.py:295
